TPU v7x, 128 devices: a whole 4x4x4 slice. The times are simulated.
128 devices in a mesh: sp: 16 (over z, x), fs: 4 (over y), tp: 2 (over core).
Axes of the slice: x: 4, y: 4, z: 4, core: 2. Of those that a mesh axis runs over, the one named last changes fastest.
Arguments:
- inputs: bfloat16 [65536, 2048], P(('fs', 'sp'), 'tp'), parts along dimension 0, may hold values from -270 to 270
- mix_gain: float32 [2048], replicated, may hold values from 0.1 to 1.9
- w_query: bfloat16 [2048, 1024], P(None, 'tp'), may hold values from -0.125 to 0.125
- w_key: bfloat16 [2048, 256], P(None, 'tp'), may hold values from -0.125 to 0.125
- w_value: bfloat16 [2048, 256], P(None, 'tp'), may hold values from -0.125 to 0.125
- query_gain: float32 [64], replicated, may hold values from 0 to 14, as said below
- key_gain: float32 [64], replicated, may hold values from 0 to 14, as said below
- sink_logit: float32 [16], P('tp'), may hold values from 3 to 7
- w_inner: bfloat16 [2048, 1024], P(None, 'tp'), may hold values from -0.125 to 0.125
- w_bmat: bfloat16 [2048, 512], P(None, 'tp'), may hold values from -0.125 to 0.125
- w_cmat: bfloat16 [2048, 512], P(None, 'tp'), may hold values from -0.125 to 0.125
- w_gate: bfloat16 [2048, 1024], P(None, 'tp'), may hold values from -0.125 to 0.125
- w_step: bfloat16 [2048, 2, 16], P(None, None, 'tp'), may hold values from -0.125 to 0.125
- conv_inner: bfloat16 [5, 1024], P(None, 'tp'), may hold values from -2.5 to 2.5
- conv_bmat: bfloat16 [5, 512], P(None, 'tp'), may hold values from -2.5 to 2.5
- conv_cmat: bfloat16 [5, 512], P(None, 'tp'), may hold values from -2.5 to 2.5
- step_bias: float32 [2, 16], P(None, 'tp'), may hold values from -1 to 1
- decay_rate: float32 [2, 16], P(None, 'tp'), may hold values from 0 to 1, as said below
- decay_offset: float32 [16384, 2, 16], P('sp', None, 'tp'), may hold values from -3 to 0, as said below
- start_state: float32 [8, 16, 64, 128], P('fs', 'tp'), parts along dimension 0, may hold values from -192 to 192
- group_gain: float32 [1024], P('tp'), may hold values from 0.1 to 1.9
- w_out_attn: bfloat16 [1024, 2048], P('tp'), may hold values from -1.5 to 1.5
- w_out_state: bfloat16 [1024, 2048], P('tp'), may hold values from -0.1875 to 0.1875
Outputs:
- mixed: bfloat16 [65536, 2048], P(('fs', 'sp', 'tp')), parts along dimension 0
There are 4 independent parts, one for each index of `fs`. A program takes and returns all parts, laid end to end along the dimension named above; an argument that names none is the same for every part. Nothing has to cross between parts.
Inputs may be any that keep to these rules, and one draw needn't show every extreme that they name: `query_gain`: positive. `key_gain`: positive. `decay_rate`: positive. `decay_offset`: never positive.
All inputs are finite; a program needn't handle non-finite values.
Results may differ from a plain program's by a relative error of at most 0.035.
Values may be sent and summed in bfloat16 or wider, within the bound.
A program may use at most 128 MiB of HBM per device.

v0:
```python
import math

import jax
import jax.numpy as jnp
import numpy as np
from jax import lax
from jax.experimental import pallas as pl
from jax.experimental.pallas import tpu as pltpu
from jax.sharding import PartitionSpec as P

D = 2048
HALF = 1024
TOK = 1024
BLK = 128
NB = 8
EPS = 1e-06
LOG2E = math.log2(math.e)
NEG = -1e30
MESH = pl.DeviceIdType.MESH
NT = (((1,), (1,)), ((), ()))
f32 = jnp.float32
bf16 = jnp.bfloat16


def iota(shape, dim):
    return lax.broadcasted_iota(jnp.int32, shape, dim)


def mm(a, b):
    return jnp.dot(a, b, preferred_element_type=f32)


def kernel(
    nsp,
    x, gain, wq, wk, wv, wi, wb, wc, wg, wst, qgain, kgain, sink, ci, cb, cc,
    prep, start, ggain, woa, wos, tabs, rows,
    out,
    X, XS, RS, WQ, WKV, WI, WBC, WG, WO, QM, KD, VD, KVS, KVR, MX, MXR, SG, TAPS,
    COS, SIN, STP, CUM, MT, INN, BA, CA, E1X, FL, BS, SS, SR, FS, FR, ES, ER, EF, ENT,
    WN, AT, PR, SST, SPR,
    lsem, wsem, xs_s, xs_r, hs_s, hs_r, ms_s, ms_r, ss_s, ss_r, fs_s, fs_r, es_s, es_r, ps_s, ps_r,
):
    me = lax.axis_index("sp")
    t = lax.axis_index("tp")
    peer = {"tp": 1 - t}
    left = {"sp": lax.rem(me + nsp - 1, nsp)}
    right = {"sp": lax.rem(me + 1, nsp)}

    def remote(src, dst, s, r, dev):
        return pltpu.make_async_remote_copy(
            src_ref=src, dst_ref=dst, send_sem=s, recv_sem=r, device_id=dev, device_id_type=MESH
        )

    barrier = pltpu.get_barrier_semaphore()
    pl.semaphore_signal(barrier, inc=1, device_id=peer, device_id_type=MESH)
    for j in range(1, nsp):
        pl.semaphore_signal(
            barrier, inc=1, device_id={"sp": lax.rem(me + j, nsp)}, device_id_type=MESH
        )

    own = pl.multiple_of(t * HALF, HALF)
    xl = pltpu.make_async_copy(x, X.at[:, pl.ds(own, HALF)], lsem)
    xl.start()
    loads = [
        (wq, WQ), (wk, WKV.at[:, 0:128]), (wv, WKV.at[:, 128:256]), (wi, WI),
        (wb, WBC.at[:, 0:256]), (wc, WBC.at[:, 256:512]), (wg, WG),
        (woa, WO.at[0:512]), (wos, WO.at[512:1024]),
    ]
    copies = [pltpu.make_async_copy(a, b, wsem.at[i]) for i, (a, b) in enumerate(loads)]
    for c in copies:
        c.start()

    for d in range(2):
        for q in range(4):
            SST[d, :, q * 128 : (q + 1) * 128] = start[d, q * 128 : (q + 1) * 128, :].T
    TAPS[0:5, 0:512] = ci[...].astype(f32)
    TAPS[0:5, 512:768] = cb[...].astype(f32)
    TAPS[0:5, 768:1024] = cc[...].astype(f32)
    ta_c = tabs[0, pl.ds(pl.multiple_of(me * NB, NB), NB), :]
    ta_s = tabs[1, pl.ds(pl.multiple_of(me * NB, NB), NB), :]
    tb_c = rows[0]
    tb_s = rows[1]
    sign = jnp.where(lax.rem(iota((1, 128), 1), 64) < 32, -1.0, 1.0).astype(f32)
    for b in range(NB):
        ac, as_ = ta_c[b : b + 1, :], ta_s[b : b + 1, :]
        COS[b * BLK : (b + 1) * BLK, :] = ac * tb_c - as_ * tb_s
        SIN[b * BLK : (b + 1) * BLK, :] = (as_ * tb_c + ac * tb_s) * sign

    pl.semaphore_wait(barrier, nsp)

    xc = []
    for h in range(2):
        c = remote(
            x.at[h * 512 : (h + 1) * 512, :],
            X.at[h * 512 : (h + 1) * 512, pl.ds(own, HALF)],
            xs_s.at[h], xs_r.at[h], peer,
        )
        c.start()
        xc.append(c)
    xl.wait()

    lane = iota((1, 128), 1)
    lo_half = lane < 64
    first_part = lax.rem(lane, 64) < 32
    g_row, g_col = iota((128, 128), 0), iota((128, 128), 1)
    head_mean = jnp.where(g_row // 64 == g_col // 64, 1.0 / 64, 0.0).astype(bf16)
    ones_lanes = jnp.ones((128, 128), bf16)

    def normed(v, gain_row, r0):
        ms = mm((v * v).astype(bf16), head_mean)
        n = v * lax.rsqrt(ms + EPS) * gain_row
        partner = jnp.where(first_part, pltpu.roll(n, 96, 1), pltpu.roll(n, 32, 1))
        return n * COS[pl.ds(r0, 128), :] + partner * SIN[pl.ds(r0, 128), :]

    sends = []
    for h in range(2):
        xc[h].wait_recv()
        h0 = h * 512

        @pl.loop(0, 8)
        def _(i):
            r = pl.multiple_of(i * 64, 64)
            v = X[pl.ds(h0 + r, 64), :].astype(f32)
            XS[pl.ds(r, 64), :] = (v * gain[...]).astype(bf16)
            ss = jnp.sum(v * v, axis=1, keepdims=True) * (1.0 / D)
            RS[pl.ds(h0 + r, 64), :] = jnp.broadcast_to(lax.rsqrt(ss + EPS), (64, 128))

        xs = XS[...]
        rs = RS[h0 : h0 + 512, :]
        if h == 0:
            copies[1].wait()
            copies[2].wait()
        kv = mm(xs, WKV[...])
        for i in range(4):
            r0 = h0 + i * 128
            rsi = rs[i * 128 : (i + 1) * 128]
            kvi = kv[i * 128 : (i + 1) * 128]
            kp = (kvi[:, 0:128] * rsi).astype(bf16).astype(f32)
            k = normed(kp, kgain[...], r0)
            v = kvi[:, 128:256] * rsi
            vb = v.astype(bf16).astype(f32)
            kb = k.astype(bf16).astype(f32)
            kr, vr = pltpu.roll(kb, 64, 1), pltpu.roll(vb, 64, 1)
            f0 = r0 + 128
            KD[0, f0 : f0 + 128, :] = jnp.where(lo_half, kb, kr).astype(bf16)
            KD[1, f0 : f0 + 128, :] = jnp.where(lo_half, kr, kb).astype(bf16)
            VD[0, f0 : f0 + 128, 0:128] = jnp.where(lo_half, vb, vr).astype(bf16)
            VD[1, f0 : f0 + 128, 0:128] = jnp.where(lo_half, vr, vb).astype(bf16)
            VD[0, f0 : f0 + 128, 128:256] = ones_lanes
            VD[1, f0 : f0 + 128, 128:256] = ones_lanes
            if r0 == 0 or r0 == 896:
                e = 0 if r0 == 0 else 1
                KVS[e, :, 0:128] = kb.astype(bf16)
                KVS[e, :, 128:256] = vb.astype(bf16)
        if h == 0:
            copies[3].wait()
            copies[4].wait()
            copies[5].wait()
        for w, base in ((WI, 0), (WBC, 512)):
            for n in range(2):
                p = mm(xs, w[:, n * 256 : (n + 1) * 256])
                for q in range(2):
                    MX[8 + h0 : 8 + h0 + 512, base + n * 256 + q * 128 : base + n * 256 + q * 128 + 128] = (
                        (p[:, q * 128 : (q + 1) * 128] * rs).astype(bf16).astype(f32)
                    )
        e = h
        dev = left if h == 0 else right
        c = remote(KVS.at[e], KVR.at[1 - e], hs_s.at[e], hs_r.at[1 - e], dev)
        c.start()
        sends.append(c)
        mrow = 8 if h == 0 else 8 + TOK - 8
        c = remote(MX.at[mrow : mrow + 8, :], MXR.at[1 - e], ms_s.at[e], ms_r.at[1 - e], dev)
        c.start()
        sends.append(c)
        if h == 0:
            copies[0].wait()
        sp_ = mm(xs, wst[...]) * rs
        for i in range(4):
            STP[h * 4 + i] = sp_[i * 128 : (i + 1) * 128].T[0:16]
        for n in range(2):
            p = mm(xs, WQ[:, n * 256 : (n + 1) * 256])
            for q in range(2):
                tile = 2 * n + q
                for i in range(4):
                    r0 = h0 + i * 128
                    qp = (
                        (p[i * 128 : (i + 1) * 128, q * 128 : (q + 1) * 128] * rs[i * 128 : (i + 1) * 128])
                        .astype(bf16)
                        .astype(f32)
                    )
                    v = normed(qp, qgain[...], r0)
                    QM[2 * tile, r0 : r0 + 128, :] = jnp.where(lo_half, v, 0.0).astype(bf16)
                    QM[2 * tile + 1, r0 : r0 + 128, :] = jnp.where(lo_half, 0.0, v).astype(bf16)
        if h == 0:
            copies[6].wait()
        for n in range(2):
            p = mm(xs, WG[:, n * 256 : (n + 1) * 256])
            for q in range(2):
                gp = (p[:, q * 128 : (q + 1) * 128] * rs).astype(bf16).astype(f32)
                SG[h0 : h0 + 512, n * 256 + q * 128 : n * 256 + (q + 1) * 128] = gp / (1.0 + jnp.exp(-gp))

    bias = prep[:, TOK : TOK + 1]
    rate = prep[:, TOK + 128 : TOK + 129]
    lane8 = iota((8, 128), 1)
    for b in range(NB):
        v = STP[b] + bias
        step = jnp.maximum(v, 0.0) + jnp.log1p(jnp.exp(-jnp.abs(v)))
        la = -rate * step + prep[:, b * BLK : (b + 1) * BLK]
        cf, cw = la[0:8], la[8:16]
        for k in (1, 2, 4, 8, 16, 32, 64):
            cf = cf + jnp.where(lane8 >= k, pltpu.roll(cf, k, 1), 0.0)
            cw = cw + jnp.where(lane8 < 128 - k, pltpu.roll(cw, 128 - k, 1), 0.0)
        cum = jnp.concatenate([cf, cw], axis=0)
        last = jnp.concatenate([cf[:, 127:128], cw[:, 0:1]], axis=0)
        e1 = jnp.exp(cum)
        e2 = step * jnp.exp(last - cum)
        STP[b] = step
        CUM[b] = cum
        MT[b * BLK : (b + 1) * BLK, :] = jnp.concatenate(
            [cum, e1, e2, jnp.zeros((80, 128), f32)], axis=0
        ).T

    def halo_in(e):
        remote(MX.at[8:16, :], MXR.at[e], ms_s.at[e], ms_r.at[e], left).wait_recv()

    ex_row, ex_col = lax.rem(iota((256, 1024), 0), 128), iota((256, 1024), 1) // 64
    SPR[0] = jnp.where(ex_row == ex_col + 16, 1.0, 0.0).astype(bf16)
    SPR[1] = jnp.where(ex_row == ex_col + 32, 1.0, 0.0).astype(bf16)

    def pre_block(b):
        r0 = pl.multiple_of(b * BLK, BLK)
        m = MT[pl.ds(r0, 128), :]
        hi = m.astype(bf16)
        lo = (m - hi.astype(f32)).astype(bf16)
        both = jnp.concatenate([hi, lo], axis=1)
        bts = [None, None]
        for ct in (4, 5, 6, 7, 0, 1, 2, 3):
            w = MX[pl.ds(r0, 144), ct * 128 : (ct + 1) * 128]
            acc = None
            for j in range(5):
                term = pltpu.roll(w, 144 - (6 + j), 0)[0:128] * TAPS[j : j + 1, ct * 128 : (ct + 1) * 128]
                acc = term if acc is None else acc + term
            act = (acc / (1.0 + jnp.exp(-acc))).astype(bf16)
            if ct >= 6:
                CA[pl.ds(r0, 128), (ct - 6) * 128 : (ct - 5) * 128] = act
            elif ct >= 4:
                BA[pl.ds(r0, 128), (ct - 4) * 128 : (ct - 3) * 128] = act
                bts[ct - 4] = act.astype(f32).T.astype(bf16)
            else:
                INN[pl.ds(r0, 128), ct * 128 : (ct + 1) * 128] = act
                g = ct // 2
                for d in range(2):
                    c0 = d * 512 + ct * 128
                    e2x = mm(both, SPR[1, :, c0 : c0 + 128])
                    loaded = (act.astype(f32) * e2x).astype(bf16)
                    BS[b, :, c0 : c0 + 128] = mm(bts[g], loaded)
        return both

    def pre_all(b):
        both = pre_block(b)
        r0 = pl.multiple_of(b * BLK, BLK)
        e1x = mm(both, SPR[0])
        return r0, e1x

    def pre_step(b):
        r0, e1x = pre_all(b)
        E1X[pl.ds(r0, 128), :] = e1x
        FL[b, 0:1, 0:512] = e1x[127:128, 0:512]
        FL[b, 0:1, 512:1024] = e1x[0:1, 512:1024]

    @pl.loop(1, 7)
    def _(b):
        pre_step(b)

    halo_in(0)
    halo_in(1)
    MX[0:8, :] = jnp.where(me == 0, 0.0, MXR[0])
    MX[8 + TOK : 16 + TOK, :] = jnp.where(me == nsp - 1, 0.0, MXR[1])

    @pl.loop(0, 2)
    def _(i):
        pre_step(i * 7)

    fd = FL[0, 0:1, :]
    for b in range(1, NB):
        fd = fd * FL[b, 0:1, :]
    FS[...] = jnp.concatenate([fd[:, i * 128 : (i + 1) * 128] for i in range(8)], axis=0)
    FR[me] = FS[...]

    def chain_out(k):
        n0 = pl.multiple_of(k * 8, 8)
        rf = jnp.zeros((8, 512), f32)
        rb = jnp.zeros((8, 512), f32)
        for b in range(NB):
            rf = FL[b, 0:1, 0:512] * rf + BS[b, pl.ds(n0, 8), 0:512]
            z = NB - 1 - b
            rb = FL[z, 0:1, 512:1024] * rb + BS[z, pl.ds(n0, 8), 512:1024]
        return jnp.concatenate([rf, rb], axis=0).astype(bf16)

    SR[me] = chain_out(me)

    @pl.loop(1, nsp)
    def _(j):
        k = lax.rem(me + j, nsp)
        SS[k] = chain_out(k)
        remote(FS, FR.at[me], fs_s.at[k], fs_r.at[me], {"sp": k}).start()
        remote(SS.at[k], SR.at[me], ss_s.at[k], ss_r.at[me], {"sp": k}).start()

    def kv_halo(e):
        remote(KVS.at[e], KVR.at[e], hs_s.at[e], hs_r.at[e], left).wait_recv()
        kb = KVR[e, :, 0:128].astype(f32)
        vb = KVR[e, :, 128:256].astype(f32)
        kr, vr = pltpu.roll(kb, 64, 1), pltpu.roll(vb, 64, 1)
        f0 = 0 if e == 0 else 128 + TOK
        KD[0, f0 : f0 + 128, :] = jnp.where(lo_half, kb, kr).astype(bf16)
        KD[1, f0 : f0 + 128, :] = jnp.where(lo_half, kr, kb).astype(bf16)
        VD[0, f0 : f0 + 128, 0:128] = jnp.where(lo_half, vb, vr).astype(bf16)
        VD[1, f0 : f0 + 128, 0:128] = jnp.where(lo_half, vr, vb).astype(bf16)
        VD[0, f0 : f0 + 128, 128:256] = ones_lanes
        VD[1, f0 : f0 + 128, 128:256] = ones_lanes

    kv_halo(0)
    kv_halo(1)

    def attend(b):
        r0 = pl.multiple_of(b * BLK, BLK)
        off_l = jnp.where((me == 0) & (b == 0), 1024, 0)
        off_r = jnp.where((me == nsp - 1) & (b == NB - 1), 1024, 0)
        keep_l = g_col >= g_row + off_l
        keep_r = g_col <= g_row - off_r
        for g in range(2):
            kk = KD[g, pl.ds(r0, 384), :]
            vv = VD[g, pl.ds(r0, 384), :]
            for pair in range(2):
                res = []
                for j in range(2):
                    h = g * 4 + pair * 2 + j
                    s = lax.dot_general(QM[h, pl.ds(r0, 128), :], kk, NT, preferred_element_type=f32)
                    sl = jnp.where(keep_l, s[:, 0:128], NEG)
                    sm = s[:, 128:256]
                    sr = jnp.where(keep_r, s[:, 256:384], NEG)
                    sk = sink[h] * LOG2E
                    m = jnp.max(jnp.maximum(jnp.maximum(sl, sm), sr), axis=1, keepdims=True)
                    m = jnp.broadcast_to(jnp.maximum(m, sk), (128, 128))
                    p = jnp.concatenate(
                        [jnp.exp2(v - m).astype(bf16) for v in (sl, sm, sr)], axis=1
                    )
                    o = mm(p, vv)
                    res.append(o[:, 0:128] / (o[:, 128:256] + jnp.exp2(sk - m)))
                tile = g * 2 + pair
                AT[pl.ds(r0, 128), tile * 128 : (tile + 1) * 128] = jnp.where(
                    lo_half, res[0], res[1]
                ).astype(bf16)

    def inside(b):
        r0 = pl.multiple_of(b * BLK, BLK)
        lower = g_row >= g_col
        diag = g_row == g_col
        for g in range(2):
            cm = CA[pl.ds(r0, 128), g * 128 : (g + 1) * 128]
            bm = BA[pl.ds(r0, 128), g * 128 : (g + 1) * 128]
            sc = lax.dot_general(cm, bm, NT, preferred_element_type=f32)
            for pair in range(2):
                tile = g * 2 + pair
                xt = INN[pl.ds(r0, 128), tile * 128 : (tile + 1) * 128].astype(f32)
                ws = []
                for j in range(2):
                    h = tile * 2 + j
                    dif = jnp.where(
                        lower,
                        MT[pl.ds(r0, 128), h : h + 1] - CUM[b, h : h + 1, :],
                        MT[pl.ds(r0, 128), 8 + h : 9 + h] - CUM[b, 8 + h : 9 + h, :],
                    )
                    sf, sb = STP[b, h : h + 1, :], STP[b, 8 + h : 9 + h, :]
                    st = jnp.where(diag, sf + sb, jnp.where(lower, sf, sb))
                    ws.append((sc * jnp.exp(dif) * st).astype(bf16))
                both = jnp.concatenate(ws, axis=1)
                xx = jnp.concatenate(
                    [jnp.where(lo_half, xt, 0.0).astype(bf16), jnp.where(lo_half, 0.0, xt).astype(bf16)],
                    axis=0,
                )
                WN[pl.ds(r0, 128), tile * 128 : (tile + 1) * 128] = mm(both, xx)

    @pl.loop(0, 5)
    def _(b):
        attend(b)

    for j in range(1, nsp):
        k = lax.rem(me + j, nsp)
        remote(FS, FR.at[k], fs_s.at[k], fs_r.at[k], {"sp": k}).wait_recv()
        remote(SS.at[k], SR.at[k], ss_s.at[k], ss_r.at[k], {"sp": k}).wait_recv()

    n0 = pl.multiple_of(me * 8, 8)

    def decay_row(d, which):
        return jnp.concatenate([FR[d, which * 4 + i : which * 4 + i + 1, :] for i in range(4)], axis=1)

    run = SST[0, pl.ds(n0, 8), :]
    for d in range(nsp):
        EF[d] = run
        run = decay_row(d, 0) * run + SR[d].astype(f32)[0:8]
    run = SST[1, pl.ds(n0, 8), :]
    for d in range(nsp - 1, -1, -1):
        ES[d] = jnp.concatenate([EF[d], run], axis=0).astype(bf16)
        run = decay_row(d, 1) * run + SR[d].astype(f32)[8:16]
    ER[me] = ES[me]

    @pl.loop(1, nsp)
    def _(j):
        k = lax.rem(me + j, nsp)
        remote(ES.at[k], ER.at[me], es_s.at[k], es_r.at[me], {"sp": k}).start()

    @pl.loop(5, NB)
    def _(b):
        attend(b)

    @pl.loop(0, NB)
    def _(b):
        inside(b)

    for j in range(1, nsp):
        k = lax.rem(me + j, nsp)
        remote(ES.at[k], ER.at[k], es_s.at[k], es_r.at[k], {"sp": k}).wait_recv()

    @pl.loop(0, 8)
    def _(i):
        n1 = pl.multiple_of(i * 16, 16)
        ea = ER[2 * i].astype(f32)
        eb = ER[2 * i + 1].astype(f32)
        rf = jnp.concatenate([ea[0:8], eb[0:8]], axis=0)
        rb = jnp.concatenate([ea[8:16], eb[8:16]], axis=0)
        for b in range(NB):
            ENT[b, pl.ds(n1, 16), 0:512] = rf.astype(bf16)
            rf = FL[b, 0:1, 0:512] * rf + BS[b, pl.ds(n1, 16), 0:512]
            z = NB - 1 - b
            ENT[z, pl.ds(n1, 16), 512:1024] = rb.astype(bf16)
            rb = FL[z, 0:1, 512:1024] * rb + BS[z, pl.ds(n1, 16), 512:1024]

    group_mean = jnp.full((256, 256), 1.0 / 256, bf16)

    def finish(b):
        r0 = pl.multiple_of(b * BLK, BLK)
        for g in range(2):
            cm = CA[pl.ds(r0, 128), g * 128 : (g + 1) * 128]
            c0, c1 = g * 256, (g + 1) * 256
            tot = (
                WN[pl.ds(r0, 128), c0:c1]
                + mm(cm, ENT[b, :, c0:c1]) * E1X[pl.ds(r0, 128), c0:c1]
                + mm(cm, ENT[b, :, 512 + c0 : 512 + c1]) * E1X[pl.ds(r0, 128), 512 + c0 : 512 + c1]
            )
            gated = tot * SG[pl.ds(r0, 128), c0:c1]
            ms = mm((gated * gated).astype(bf16), group_mean)
            AT[pl.ds(r0, 128), 512 + c0 : 512 + c1] = (
                gated * lax.rsqrt(ms + EPS) * ggain[0:1, c0:c1]
            ).astype(bf16)

    copies[7].wait()
    copies[8].wait()
    other = pl.multiple_of((1 - t) * 512, 512)
    mine = pl.multiple_of(t * 512, 512)
    pc = []

    @pl.loop(0, 4)
    def _(i):
        finish((1 - t) * 4 + i)

    for n in range(4):
        XS[:, n * 512 : (n + 1) * 512] = mm(
            AT[pl.ds(other, 512), :], WO[:, n * 512 : (n + 1) * 512]
        ).astype(bf16)
        c = remote(
            XS.at[:, n * 512 : (n + 1) * 512], PR.at[:, n * 512 : (n + 1) * 512],
            ps_s.at[n], ps_r.at[n], peer,
        )
        c.start()
        pc.append(c)

    @pl.loop(0, 4)
    def _(i):
        finish(t * 4 + i)

    for n in range(4):
        p = mm(AT[pl.ds(mine, 512), :], WO[:, n * 512 : (n + 1) * 512]).astype(bf16).astype(f32)
        pc[n].wait_recv()
        out[:, n * 512 : (n + 1) * 512] = (
            p + PR[:, n * 512 : (n + 1) * 512].astype(f32)
        ).astype(bf16)

    for c in xc + sends + pc:
        c.wait_send()

    @pl.loop(1, nsp)
    def _(j):
        k = lax.rem(me + j, nsp)
        remote(FS, FR.at[me], fs_s.at[k], fs_r.at[me], {"sp": k}).wait_send()
        remote(SS.at[k], SR.at[me], ss_s.at[k], ss_r.at[me], {"sp": k}).wait_send()
        remote(ES.at[k], ER.at[me], es_s.at[k], es_r.at[me], {"sp": k}).wait_send()


def tables(blocks):
    freq = 10000.0 ** (-(np.arange(128) % 32) / 32.0)
    a = np.arange(blocks)[:, None] * 128.0 * freq[None, :]
    r = np.arange(128)[:, None] * freq[None, :]
    return (
        np.stack([np.cos(a), np.sin(a)]).astype(np.float32),
        np.stack([np.cos(r), np.sin(r)]).astype(np.float32),
    )


def local(
    nsp, inputs, mix_gain, w_query, w_key, w_value, query_gain, key_gain, sink_logit, w_inner, w_bmat, w_cmat,
    w_gate, w_step, conv_inner, conv_bmat, conv_cmat, step_bias, decay_rate, decay_offset, start_state,
    group_gain, w_out_attn, w_out_state,
):
    wst = jnp.pad(w_step.reshape(D, 16), ((0, 0), (0, 112)))
    qgain = (jnp.tile(query_gain, 2) * (LOG2E / 8.0)).reshape(1, 128)
    kgain = jnp.tile(key_gain, 2).reshape(1, 128)
    off = jnp.transpose(decay_offset, (1, 2, 0)).reshape(16, TOK)
    prep = jnp.concatenate(
        [
            off,
            jnp.broadcast_to(step_bias.reshape(16, 1), (16, 128)),
            jnp.broadcast_to(decay_rate.reshape(16, 1), (16, 128)),
        ],
        axis=1,
    )
    tabs, rows = tables(nsp * NB)
    hbm = pl.BlockSpec(memory_space=pl.ANY)
    vm = pl.BlockSpec(memory_space=pltpu.VMEM)
    sm = pl.BlockSpec(memory_space=pltpu.SMEM)
    V = pltpu.VMEM
    dma = pltpu.SemaphoreType.DMA
    return pl.pallas_call(
        lambda *refs: kernel(nsp, *refs),
        name="layer",
        out_shape=jax.ShapeDtypeStruct((TOK // 2, D), bf16),
        in_specs=[hbm, vm, hbm, hbm, hbm, hbm, hbm, hbm, hbm, vm, vm, vm, sm, vm, vm, vm, vm, vm, vm, hbm, hbm, vm, vm],
        out_specs=vm,
        scratch_shapes=[
            V((TOK, D), bf16), V((512, D), bf16), V((TOK, 128), f32),
            V((D, 512), bf16), V((D, 256), bf16), V((D, 512), bf16), V((D, 512), bf16), V((D, 512), bf16),
            V((1024, D), bf16),
            V((8, TOK, 128), bf16), V((2, TOK + 256, 128), bf16), V((2, TOK + 256, 256), bf16),
            V((2, 128, 256), bf16), V((2, 128, 256), bf16),
            V((TOK + 16, 1024), f32), V((2, 8, 1024), f32), V((TOK, 512), f32), V((8, 1024), f32),
            V((TOK, 128), f32), V((TOK, 128), f32),
            V((NB, 16, 128), f32), V((NB, 16, 128), f32), V((TOK, 128), f32),
            V((TOK, 512), bf16), V((TOK, 256), bf16), V((TOK, 256), bf16),
            V((TOK, 1024), f32), V((NB, 8, 1024), f32), V((NB, 128, 1024), f32),
            V((nsp, 16, 512), bf16), V((nsp, 16, 512), bf16), V((8, 128), f32), V((nsp, 8, 128), f32),
            V((nsp, 16, 512), bf16), V((nsp, 16, 512), bf16), V((nsp, 8, 512), f32),
            V((NB, 128, 1024), bf16),
            V((TOK, 512), f32), V((TOK, 1024), bf16), V((512, D), bf16), V((2, 128, 512), f32), V((2, 256, 1024), bf16),
            dma, dma((9,)), dma((2,)), dma((2,)), dma((2,)), dma((2,)), dma((2,)), dma((2,)),
            dma((nsp,)), dma((nsp,)), dma((nsp,)), dma((nsp,)), dma((nsp,)), dma((nsp,)), dma((4,)), dma((4,)),
        ],
        compiler_params=pltpu.CompilerParams(
            collective_id=0, has_side_effects=True, vmem_limit_bytes=64 * 1024 * 1024 - 65536
        ),
    )(
        inputs, mix_gain.reshape(1, D), w_query, w_key, w_value, w_inner, w_bmat, w_cmat, w_gate, wst,
        qgain, kgain, sink_logit, conv_inner, conv_bmat, conv_cmat, prep, start_state.reshape(2, 512, 128),
        group_gain.reshape(1, 512), w_out_attn, w_out_state, jnp.asarray(tabs), jnp.asarray(rows),
    )


def solution(mesh):
    nsp = mesh.shape["sp"]
    return jax.shard_map(
        lambda *args: local(nsp, *args),
        mesh=mesh,
        in_specs=(
            P(("fs", "sp"), "tp"), P(), P(None, "tp"), P(None, "tp"), P(None, "tp"), P(), P(), P("tp"),
            P(None, "tp"), P(None, "tp"), P(None, "tp"), P(None, "tp"), P(None, None, "tp"),
            P(None, "tp"), P(None, "tp"), P(None, "tp"), P(None, "tp"), P(None, "tp"),
            P("sp", None, "tp"), P("fs", "tp", None, None), P("tp"), P("tp", None), P("tp", None),
        ),
        out_specs=P(("fs", "sp", "tp"), None),
        check_vma=False,
    )
```

profile of v0, /device:TPU:1, one launch (start us, length us, event | category | flops | bytes accessed | tf_op | source)
XLA Modules:
  0.0 81.6 jit_solution(8258140277353417865)
XLA Ops:
  0.0 0.7 broadcast_multiply_fusion
  0.7 0.6 mul.19.refs_10_
  1.3 0.8 broadcast_in_dim.14
  2.0 0.8 broadcast_in_dim.16
  2.8 0.7 tile.5
  3.4 0.6 reshape_tile.3.refs_11_
  4.0 0.1 broadcast_in_dim.17
  4.1 0.1 broadcast_in_dim.15
  4.2 1.5 %pad_maximum_fusion.refs_16_ = f32[16,1280]{1,0:T(8,128)} fusion(f32[16,128]{1,0:T(8,128)S(1)} %broadcast_in_dim.17, f32[16,128]{1,0:T(8,128)S(1)} %broadcast_in_dim.15, f32[16,1024]{1,0:T(8,128)} %bitcast.9), kind=kLoop, calls=%fused_computation | loop fusion | flops 40960 | bytes 163840 | tf_op jit(solution)/shard_map/concatenate | solution.py:519
  5.7 1.1 %copy.27 = bf16[2048,16]{1,0:T(8,128)(2,1)S(1)} copy(bf16[2048,16]{0,1:T(8,128)(2,1)} %bitcast.8) | data formatting | bytes 131072 | tf_op jit(solution)/shard_map/reshape | solution.py:515
  6.8 0.9 %pad.4.refs_9_ = bf16[2048,128]{1,0:T(8,128)(2,1)} pad(bf16[2048,16]{1,0:T(8,128)(2,1)S(1)} %copy.27, bf16[]{:T(256)} %constant.3.clone.1), padding=0_0x0_112 | pad | bytes 589826 | tf_op jit(solution)/shard_map/jit(_pad)/pad | solution.py:515
  7.7 70.7 %layer.1 = bf16[512,2048]{1,0:T(8,128)(2,1)} custom-call(bf16[1024,1024]{1,0:T(8,128)(2,1)} %refs_0_.1, f32[1,2048]{1,0:T(1,128)} %bitcast.10, bf16[2048,512]{1,0:T(8,128)(2,1)} %refs_2_.1, bf16[2048,128]{1,0:T(8,128)(2,1)} %refs_3_.1, bf16[2048,128]{1,0:T(8,128)(2,1)} %refs_4_.1, bf16[2048,512]{1,0:T(8,128)(2,1)} %refs_5_.1, bf16[2048,256]{1,0:T(8,128)(2,1)} %refs_6_.1, ...), custom_call_target="tpu_custom_call" | custom-call | tf_op jit(solution)/shard_map/layer/pallas_call | solution.py:533
  78.4 3.2 %copy.29 = bf16[512,2048]{1,0:T(8,128)(2,1)} copy(bf16[512,2048]{1,0:T(8,128)(2,1)} %layer.1) | data formatting | bytes 4194304
  (1 shorter events, 0.0 us)
where the time goes:
time: 81.9 us; the launch traced here: 81.6 us
  Pallas kernels  70.7 us (86%)
  local copies, waits for them, and re-layouts  8.68 us (11%)
  other arithmetic  2.14 us (3%)
    pallas_call x1, Pallas kernels, local(): pl.pallas_call(lambda *refs: kernel(nsp, *refs), name='layer', out_shape=...  70.7 us
    unnamed x1, local copies, waits for them, and re-layouts  3.16 us

commit v1 on v0

v1 whole, which is shorter than its diff:
```python
import math

import jax
import jax.numpy as jnp
import numpy as np
from jax import lax
from jax.experimental import pallas as pl
from jax.experimental.pallas import tpu as pltpu
from jax.sharding import PartitionSpec as P

D = 2048
HALF = 1024
TOK = 1024
BLK = 128
NB = 8
EPS = 1e-06
LOG2E = math.log2(math.e)
NEG = -1e30
MESH = pl.DeviceIdType.MESH
NT = (((1,), (1,)), ((), ()))
f32 = jnp.float32
bf16 = jnp.bfloat16


def iota(shape, dim):
    return lax.broadcasted_iota(jnp.int32, shape, dim)


def mm(a, b):
    return jnp.dot(a, b, preferred_element_type=f32)


def silu(v):
    h = 0.5 * v
    return h + h * jnp.tanh(h)


def kernel(
    nsp,
    x, gain, wq, wk, wv, wi, wb, wc, wg, wst, qgain, kgain, sink, ci, cb, cc,
    bias, rate, off, start, ggain, woa, wos, tabs, rows,
    out,
    XO0, XO1, XP0, XP1, RS, WQ, WKV, WI, WBC, WG, WO, WST, QM, KD, VD, KVS, KVR, MX, MXR, SG, TAPS,
    COS, SIN, STP, CUM, MT, INN, BA, CA, E1X, FL, BS, SS, SR, FS, FR, ES, ER, EF, ENT,
    WN, AT, PR, SST, SPR, HM, STV, TBV, RWV,
    lsem, wsem, xs_s, xs_r, hs_s, hs_r, ms_s, ms_r, ss_s, ss_r, fs_s, fs_r, es_s, es_r, ps_s, ps_r, osem,
):
    me = lax.axis_index("sp")
    t = lax.axis_index("tp")
    peer = {"tp": 1 - t}
    left = {"sp": lax.rem(me + nsp - 1, nsp)}
    right = {"sp": lax.rem(me + 1, nsp)}
    XO, XP = (XO0, XO1), (XP0, XP1)

    def remote(src, dst, s, r, dev):
        return pltpu.make_async_remote_copy(
            src_ref=src, dst_ref=dst, send_sem=s, recv_sem=r, device_id=dev, device_id_type=MESH
        )

    barrier = pltpu.get_barrier_semaphore()
    pl.semaphore_signal(barrier, inc=1, device_id=peer, device_id_type=MESH)
    for j in range(1, nsp):
        pl.semaphore_signal(
            barrier, inc=1, device_id={"sp": lax.rem(me + j, nsp)}, device_id_type=MESH
        )

    own = pl.multiple_of(t * HALF, HALF)
    oth = pl.multiple_of((1 - t) * HALF, HALF)
    xl = [pltpu.make_async_copy(x.at[h * 512 : (h + 1) * 512, :], XO[h], lsem.at[h]) for h in range(2)]
    small = [
        pltpu.make_async_copy(start, STV, lsem.at[2]),
        pltpu.make_async_copy(tabs.at[:, pl.ds(pl.multiple_of(me * NB, NB), NB), :], TBV, lsem.at[3]),
        pltpu.make_async_copy(rows, RWV, lsem.at[4]),
    ]
    pieces = [(wk, WKV, 0, 128), (wv, WKV, 128, 128), (wi, WI, 0, 512), (wb, WBC, 0, 256), (wc, WBC, 256, 256)]
    first = [
        pltpu.make_async_copy(w.at[pl.ds(own, HALF), :], d.at[pl.ds(own, HALF), c0 : c0 + n], wsem.at[i])
        for i, (w, d, c0, n) in enumerate(pieces)
    ]
    second = [
        pltpu.make_async_copy(w.at[pl.ds(oth, HALF), :], d.at[pl.ds(oth, HALF), c0 : c0 + n], wsem.at[5 + i])
        for i, (w, d, c0, n) in enumerate(pieces)
    ]
    third = [
        pltpu.make_async_copy(wq, WQ, wsem.at[10]),
        pltpu.make_async_copy(wg, WG, wsem.at[11]),
        pltpu.make_async_copy(woa, WO.at[0:512], wsem.at[12]),
        pltpu.make_async_copy(wos, WO.at[512:1024], wsem.at[13]),
    ]
    for c in [xl[0]] + first + [xl[1]] + small + second + third:
        c.start()

    lane = iota((1, 128), 1)
    lo_half = lane < 64
    first_part = lax.rem(lane, 64) < 32
    g_row, g_col = iota((128, 128), 0), iota((128, 128), 1)
    ones_lanes = jnp.ones((128, 128), bf16)
    HM[...] = jnp.where(iota((256, 256), 0) // 64 == iota((256, 256), 1) // 64, 1.0 / 64, 0.0).astype(bf16)
    WST[...] = jnp.zeros((128, D), bf16)
    WST[0:16, :] = wst[...]
    TAPS[0:5, 0:512] = ci[...].astype(f32)
    TAPS[0:5, 512:768] = cb[...].astype(f32)
    TAPS[0:5, 768:1024] = cc[...].astype(f32)
    qg = jnp.concatenate([qgain[...], qgain[...]], axis=1) * (LOG2E / 8.0)
    kg = jnp.concatenate([kgain[...], kgain[...]], axis=1)

    def scale(ref, off_, h, begin):
        g = gain[0:1, pl.ds(off_, HALF)]
        for i in range(8):
            r = i * 64
            v = ref[r : r + 64, :].astype(f32)
            ref[r : r + 64, :] = (v * g).astype(bf16)
            ss = jnp.broadcast_to(jnp.sum(v * v, axis=1, keepdims=True), (64, 128))
            if begin:
                RS[h, r : r + 64, :] = ss
            else:
                RS[h, r : r + 64, :] = lax.rsqrt((RS[h, r : r + 64, :] + ss) * (1.0 / D) + EPS)

    mixed_tiles = [(WI, 0), (WI, 256), (WBC, 0), (WBC, 256)]

    def part_one(h):
        rows_ = slice(h * 512, (h + 1) * 512)
        xs = XO[h][...]
        WN[rows_, 0:256] = mm(xs, WKV[pl.ds(own, HALF), :])
        WN[rows_, 256:384] = lax.dot_general(xs, WST[:, pl.ds(own, HALF)], NT, preferred_element_type=f32)
        if h == 0:
            for c in first[2:]:
                c.wait()
        for n, (w, c0) in enumerate(mixed_tiles):
            E1X[rows_, n * 256 : (n + 1) * 256] = mm(xs, w[pl.ds(own, HALF), c0 : c0 + 256])

    xl[0].wait()
    scale(XO[0], own, 0, True)
    first[0].wait()
    first[1].wait()
    part_one(0)
    with jax.named_scope("w_barrier"):
        pl.semaphore_wait(barrier, nsp)
    xc = []
    for h in range(2):
        c = remote(x.at[h * 512 : (h + 1) * 512, :], XP[h], xs_s.at[h], xs_r.at[h], peer)
        c.start()
        xc.append(c)
    xl[1].wait()
    scale(XO[1], own, 1, True)
    part_one(1)

    for c in small:
        c.wait()
    for d in range(2):
        for q in range(4):
            SST[d, :, q * 128 : (q + 1) * 128] = STV[d, q * 128 : (q + 1) * 128, :].T
    sign = jnp.where(first_part, -1.0, 1.0).astype(f32)
    for b in range(NB):
        ac, as_ = TBV[0, b : b + 1, :], TBV[1, b : b + 1, :]
        COS[b * BLK : (b + 1) * BLK, :] = ac * RWV[0] - as_ * RWV[1]
        SIN[b * BLK : (b + 1) * BLK, :] = (as_ * RWV[0] + ac * RWV[1]) * sign
    for d in range(2):
        ex_row, ex_col = lax.rem(iota((256, 1024), 0), 128), iota((256, 1024), 1) // 64
        SPR[d] = jnp.where(ex_row == ex_col + 16 * (d + 1), 1.0, 0.0).astype(bf16)

    def rotated(n, r0):
        partner = jnp.where(first_part, pltpu.roll(n, 96, 1), pltpu.roll(n, 32, 1))
        return n * COS[r0 : r0 + 128, :] + partner * SIN[r0 : r0 + 128, :]

    def keep_kv(kb, vb, f0):
        kr, vr = pltpu.roll(kb, 64, 1), pltpu.roll(vb, 64, 1)
        KD[0, f0 : f0 + 128, :] = jnp.where(lo_half, kb, kr).astype(bf16)
        KD[1, f0 : f0 + 128, :] = jnp.where(lo_half, kr, kb).astype(bf16)
        VD[0, f0 : f0 + 128, 0:128] = jnp.where(lo_half, vb, vr).astype(bf16)
        VD[1, f0 : f0 + 128, 0:128] = jnp.where(lo_half, vr, vb).astype(bf16)
        VD[0, f0 : f0 + 128, 128:256] = ones_lanes
        VD[1, f0 : f0 + 128, 128:256] = ones_lanes

    sends = []

    def part_two(h):
        h0 = h * 512
        rows_ = slice(h0, h0 + 512)
        xs = XP[h][...]
        for n, (w, c0) in enumerate(mixed_tiles):
            p = mm(xs, w[pl.ds(oth, HALF), c0 : c0 + 256])
            for q in range(2):
                ct = 2 * n + q
                MX[ct, 8 + h0 : 8 + h0 + 512, :] = (
                    ((p[:, q * 128 : (q + 1) * 128] + E1X[rows_, ct * 128 : (ct + 1) * 128]) * RS[h])
                    .astype(bf16)
                    .astype(f32)
                )
        kv = mm(xs, WKV[pl.ds(oth, HALF), :])
        sp_ = lax.dot_general(xs, WST[:, pl.ds(oth, HALF)], NT, preferred_element_type=f32)
        for i in range(4):
            sub = slice(i * 128, (i + 1) * 128)
            STP[h * 4 + i] = ((sp_[sub] + WN[h0 + i * 128 : h0 + (i + 1) * 128, 256:384]) * RS[h, sub, :]).T[0:16]
        kp = ((kv[:, 0:128] + WN[rows_, 0:128]) * RS[h]).astype(bf16).astype(f32)
        vb = ((kv[:, 128:256] + WN[rows_, 128:256]) * RS[h]).astype(bf16).astype(f32)
        ms = mm((kp * kp).astype(bf16), HM[0:128, 0:128])
        for i in range(4):
            r0 = h0 + i * 128
            sub = slice(i * 128, (i + 1) * 128)
            k = rotated(kp[sub] * lax.rsqrt(ms[sub] + EPS) * kg, r0)
            kb = k.astype(bf16).astype(f32)
            keep_kv(kb, vb[sub], r0 + 128)
            if r0 == 0 or r0 == 896:
                KVS[h, :, 0:128] = kb.astype(bf16)
                KVS[h, :, 128:256] = vb[sub].astype(bf16)
        dev = left if h == 0 else right
        mrow = 8 if h == 0 else TOK
        c = remote(MX.at[:, mrow : mrow + 8, :], MXR.at[1 - h], ms_s.at[h], ms_r.at[1 - h], dev)
        c.start()
        sends.append(c)
        c = remote(KVS.at[h], KVR.at[1 - h], hs_s.at[h], hs_r.at[1 - h], dev)
        c.start()
        sends.append(c)

    for h in range(2):
        with jax.named_scope(f"w_x{h}"):
            xc[h].wait_recv()
        if h == 0:
            with jax.named_scope("w_w2"):
                for c in second:
                    c.wait()
        scale(XP[h], oth, h, False)
        part_two(h)

    with jax.named_scope("w_qg"):
        third[0].wait()
        third[1].wait()

    row16 = iota((16, 128), 0)
    bias_c = jnp.zeros((16, 128), f32)
    rate_c = jnp.zeros((16, 128), f32)
    for r in range(16):
        bias_c = jnp.where(row16 == r, bias[r // 8, r % 8], bias_c)
        rate_c = jnp.where(row16 == r, rate[r // 8, r % 8], rate_c)
    lane8 = iota((8, 128), 1)

    def steps(b):
        v = STP[b] + bias_c
        step = jnp.maximum(v, 0.0) + jnp.log1p(jnp.exp(-jnp.abs(v)))
        la = (-rate_c * step + off[:, b * BLK : (b + 1) * BLK]) * LOG2E
        cf, cw = la[0:8], la[8:16]
        for k in (1, 2, 4, 8, 16, 32, 64):
            cf = cf + jnp.where(lane8 >= k, pltpu.roll(cf, k, 1), 0.0)
            cw = cw + jnp.where(lane8 < 128 - k, pltpu.roll(cw, 128 - k, 1), 0.0)
        cum = jnp.concatenate([cf, cw], axis=0)
        last = jnp.concatenate([cf[:, 127:128], cw[:, 0:1]], axis=0)
        e1 = jnp.exp2(cum)
        e2 = step * jnp.exp2(last - cum)
        STP[b] = step
        CUM[b] = cum
        MT[b * BLK : (b + 1) * BLK, :] = jnp.concatenate(
            [cum, e1, e2, jnp.zeros((80, 128), f32)], axis=0
        ).T

    def pre_block(b):
        r0 = b * BLK
        m = MT[r0 : r0 + 128, :]
        hi = m.astype(bf16)
        lo = (m - hi.astype(f32)).astype(bf16)
        both = jnp.concatenate([hi, lo], axis=1)
        bts = [None, None]
        for ct in (4, 5, 6, 7, 0, 1, 2, 3):
            acc = None
            for j in range(5):
                term = MX[ct, r0 + 6 + j : r0 + 6 + j + 128, :] * TAPS[j : j + 1, ct * 128 : (ct + 1) * 128]
                acc = term if acc is None else acc + term
            act = silu(acc).astype(bf16)
            if ct >= 6:
                CA[r0 : r0 + 128, (ct - 6) * 128 : (ct - 5) * 128] = act
            elif ct >= 4:
                BA[r0 : r0 + 128, (ct - 4) * 128 : (ct - 3) * 128] = act
                bts[ct - 4] = act.astype(f32).T.astype(bf16)
            else:
                INN[r0 : r0 + 128, ct * 128 : (ct + 1) * 128] = act
                if ct % 2 == 0:
                    continue
                g = ct // 2
                for d in range(2):
                    c0 = d * 512 + g * 256
                    e2x = mm(both, SPR[1, :, c0 : c0 + 256])
                    loaded = (INN[r0 : r0 + 128, g * 256 : (g + 1) * 256].astype(f32) * e2x).astype(bf16)
                    BS[b, :, c0 : c0 + 256] = mm(bts[g], loaded)
        e1x = mm(both, SPR[0])
        E1X[r0 : r0 + 128, :] = e1x
        FL[b, 0:1, 0:512] = e1x[127:128, 0:512]
        FL[b, 0:1, 512:1024] = e1x[0:1, 512:1024]

    def query_tile(h, n):
        h0 = h * 512
        p = mm(XO[h][...], WQ[pl.ds(own, HALF), n * 256 : (n + 1) * 256]) + mm(
            XP[h][...], WQ[pl.ds(oth, HALF), n * 256 : (n + 1) * 256]
        )
        qp = [(p[:, q * 128 : (q + 1) * 128] * RS[h]).astype(bf16).astype(f32) for q in range(2)]
        ms = mm(jnp.concatenate([(v * v).astype(bf16) for v in qp], axis=1), HM[...])
        for q in range(2):
            for i in range(4):
                sub = slice(i * 128, (i + 1) * 128)
                v = rotated(qp[q][sub] * lax.rsqrt(ms[sub, q * 128 : (q + 1) * 128] + EPS) * qg, h0 + i * 128)
                QM[n, h * 4 + i, q * 256 : q * 256 + 128, :] = jnp.where(lo_half, v, 0.0).astype(bf16)
                QM[n, h * 4 + i, q * 256 + 128 : q * 256 + 256, :] = jnp.where(lo_half, 0.0, v).astype(bf16)

    def gate_tile(h, n):
        h0 = h * 512
        p = mm(XO[h][...], WG[pl.ds(own, HALF), n * 256 : (n + 1) * 256]) + mm(
            XP[h][...], WG[pl.ds(oth, HALF), n * 256 : (n + 1) * 256]
        )
        for q in range(2):
            gp = (p[:, q * 128 : (q + 1) * 128] * RS[h]).astype(bf16).astype(f32)
            SG[h0 : h0 + 512, n * 256 + q * 128 : n * 256 + (q + 1) * 128] = silu(gp)

    for b in range(NB):
        steps(b)
    for i, b in enumerate((1, 2, 3, 4, 5, 6, 7, 0)):
        if i == 6:
            with jax.named_scope("w_halo"):
                for e in range(2):
                    remote(MX.at[:, 8:16, :], MXR.at[e], ms_s.at[e], ms_r.at[e], left).wait_recv()
            MX[:, 0:8, :] = jnp.where(me == 0, 0.0, MXR[0])
            MX[:, 8 + TOK : 16 + TOK, :] = jnp.where(me == nsp - 1, 0.0, MXR[1])
        (query_tile if i < 4 else gate_tile)((i // 2) % 2, i % 2)
        pre_block(b)

    fd = FL[0, 0:1, :]
    for b in range(1, NB):
        fd = fd * FL[b, 0:1, :]
    FS[...] = jnp.concatenate([fd[:, i * 128 : (i + 1) * 128] for i in range(8)], axis=0)
    FR[me] = FS[...]

    def chain_out(k):
        n0 = pl.multiple_of(k * 8, 8)
        rf = jnp.zeros((8, 512), f32)
        rb = jnp.zeros((8, 512), f32)
        for b in range(NB):
            rf = FL[b, 0:1, 0:512] * rf + BS[b, pl.ds(n0, 8), 0:512]
            z = NB - 1 - b
            rb = FL[z, 0:1, 512:1024] * rb + BS[z, pl.ds(n0, 8), 512:1024]
        return jnp.concatenate([rf, rb], axis=0).astype(bf16)

    SR[me] = chain_out(me)

    @pl.loop(1, nsp)
    def _(j):
        k = lax.rem(me + j, nsp)
        SS[k] = chain_out(k)
        remote(FS, FR.at[me], fs_s.at[k], fs_r.at[me], {"sp": k}).start()
        remote(SS.at[k], SR.at[me], ss_s.at[k], ss_r.at[me], {"sp": k}).start()

    with jax.named_scope("w_kvh"):
        for e in range(2):
            remote(KVS.at[e], KVR.at[e], hs_s.at[e], hs_r.at[e], left).wait_recv()
    for e in range(2):
        keep_kv(
            KVR[e, :, 0:128].astype(f32), KVR[e, :, 128:256].astype(f32), 0 if e == 0 else 128 + TOK
        )

    def attend(b):
        r0 = pl.multiple_of(b * BLK, BLK)
        off_l = jnp.where((me == 0) & (b == 0), 1024, 0)
        off_r = jnp.where((me == nsp - 1) & (b == NB - 1), 1024, 0)
        keep_l = g_col >= g_row + off_l
        keep_r = g_col <= g_row - off_r
        for g in range(2):
            kk = KD[g, pl.ds(r0, 384), :]
            vv = VD[g, pl.ds(r0, 384), :]
            s = lax.dot_general(QM[g, b], kk, NT, preferred_element_type=f32)
            ps, ms = [], []
            for j in range(4):
                sj = s[j * 128 : (j + 1) * 128]
                sl = jnp.where(keep_l, sj[:, 0:128], NEG)
                sm = sj[:, 128:256]
                sr = jnp.where(keep_r, sj[:, 256:384], NEG)
                sk = sink[g * 4 + j] * LOG2E
                m = jnp.max(jnp.maximum(jnp.maximum(sl, sm), sr), axis=1, keepdims=True)
                m = jnp.broadcast_to(jnp.maximum(m, sk), (128, 128))
                ps.append(jnp.concatenate([jnp.exp2(v - m).astype(bf16) for v in (sl, sm, sr)], axis=1))
                ms.append(jnp.exp2(sk - m))
            o = mm(jnp.concatenate(ps, axis=0), vv)
            res = [
                o[j * 128 : (j + 1) * 128, 0:128] / (o[j * 128 : (j + 1) * 128, 128:256] + ms[j]) for j in range(4)
            ]
            for pair in range(2):
                tile = g * 2 + pair
                AT[pl.ds(r0, 128), tile * 128 : (tile + 1) * 128] = jnp.where(
                    lo_half, res[2 * pair], res[2 * pair + 1]
                ).astype(bf16)

    def inside(b):
        r0 = pl.multiple_of(b * BLK, BLK)
        lower = g_row >= g_col
        diag = g_row == g_col
        for g in range(2):
            cm = CA[pl.ds(r0, 128), g * 128 : (g + 1) * 128]
            bm = BA[pl.ds(r0, 128), g * 128 : (g + 1) * 128]
            sc = lax.dot_general(cm, bm, NT, preferred_element_type=f32)
            for pair in range(2):
                tile = g * 2 + pair
                xt = INN[pl.ds(r0, 128), tile * 128 : (tile + 1) * 128].astype(f32)
                ws = []
                for j in range(2):
                    h = tile * 2 + j
                    dif = jnp.where(
                        lower,
                        MT[pl.ds(r0, 128), h : h + 1] - CUM[b, h : h + 1, :],
                        MT[pl.ds(r0, 128), 8 + h : 9 + h] - CUM[b, 8 + h : 9 + h, :],
                    )
                    sf, sb = STP[b, h : h + 1, :], STP[b, 8 + h : 9 + h, :]
                    st = jnp.where(diag, sf + sb, jnp.where(lower, sf, sb))
                    ws.append((sc * jnp.exp2(dif) * st).astype(bf16))
                both = jnp.concatenate(ws, axis=1)
                xx = jnp.concatenate(
                    [jnp.where(lo_half, xt, 0.0).astype(bf16), jnp.where(lo_half, 0.0, xt).astype(bf16)],
                    axis=0,
                )
                WN[pl.ds(r0, 128), tile * 128 : (tile + 1) * 128] = mm(both, xx)

    @pl.loop(0, 5)
    def _(b):
        attend(b)
        inside(b)

    with jax.named_scope("w_s"):
        for j in range(1, nsp):
            k = lax.rem(me + j, nsp)
            remote(FS, FR.at[k], fs_s.at[k], fs_r.at[k], {"sp": k}).wait_recv()
            remote(SS.at[k], SR.at[k], ss_s.at[k], ss_r.at[k], {"sp": k}).wait_recv()

    n0 = pl.multiple_of(me * 8, 8)

    def decay_row(d, which):
        return jnp.concatenate([FR[d, which * 4 + i : which * 4 + i + 1, :] for i in range(4)], axis=1)

    run = SST[0, pl.ds(n0, 8), :]
    for d in range(nsp):
        EF[d] = run
        run = decay_row(d, 0) * run + SR[d].astype(f32)[0:8]
    run = SST[1, pl.ds(n0, 8), :]
    for d in range(nsp - 1, -1, -1):
        ES[d] = jnp.concatenate([EF[d], run], axis=0).astype(bf16)
        run = decay_row(d, 1) * run + SR[d].astype(f32)[8:16]
    ER[me] = ES[me]

    @pl.loop(1, nsp)
    def _(j):
        k = lax.rem(me + j, nsp)
        remote(ES.at[k], ER.at[me], es_s.at[k], es_r.at[me], {"sp": k}).start()

    @pl.loop(5, NB)
    def _(b):
        attend(b)
        inside(b)

    with jax.named_scope("w_e"):
        for j in range(1, nsp):
            k = lax.rem(me + j, nsp)
            remote(ES.at[k], ER.at[k], es_s.at[k], es_r.at[k], {"sp": k}).wait_recv()

    @pl.loop(0, 8)
    def _(i):
        n1 = pl.multiple_of(i * 16, 16)
        ea = ER[2 * i].astype(f32)
        eb = ER[2 * i + 1].astype(f32)
        rf = jnp.concatenate([ea[0:8], eb[0:8]], axis=0)
        rb = jnp.concatenate([ea[8:16], eb[8:16]], axis=0)
        for b in range(NB):
            ENT[b, pl.ds(n1, 16), 0:512] = rf.astype(bf16)
            rf = FL[b, 0:1, 0:512] * rf + BS[b, pl.ds(n1, 16), 0:512]
            z = NB - 1 - b
            ENT[z, pl.ds(n1, 16), 512:1024] = rb.astype(bf16)
            rb = FL[z, 0:1, 512:1024] * rb + BS[z, pl.ds(n1, 16), 512:1024]

    group_mean = jnp.full((256, 256), 1.0 / 256, bf16)

    def finish(b):
        r0 = pl.multiple_of(b * BLK, BLK)
        for g in range(2):
            cm = CA[pl.ds(r0, 128), g * 128 : (g + 1) * 128]
            c0, c1 = g * 256, (g + 1) * 256
            tot = (
                WN[pl.ds(r0, 128), c0:c1]
                + mm(cm, ENT[b, :, c0:c1]) * E1X[pl.ds(r0, 128), c0:c1]
                + mm(cm, ENT[b, :, 512 + c0 : 512 + c1]) * E1X[pl.ds(r0, 128), 512 + c0 : 512 + c1]
            )
            gated = tot * SG[pl.ds(r0, 128), c0:c1]
            ms = mm((gated * gated).astype(bf16), group_mean)
            AT[pl.ds(r0, 128), 512 + c0 : 512 + c1] = (
                gated * lax.rsqrt(ms + EPS) * ggain[0:1, c0:c1]
            ).astype(bf16)

    with jax.named_scope("w_wo"):
        third[2].wait()
        third[3].wait()
    other = pl.multiple_of((1 - t) * 512, 512)
    mine = pl.multiple_of(t * 512, 512)
    pc = []
    oc = []

    @pl.loop(0, 4)
    def _(i):
        finish((1 - t) * 4 + i)

    for n in range(8):
        dst = (XO0, XP0)[n // 4]
        c0 = (n % 4) * 256
        dst[:, c0 : c0 + 256] = mm(AT[pl.ds(other, 512), :], WO[:, n * 256 : (n + 1) * 256]).astype(bf16)
        if n % 2 == 1:
            c = remote(
                dst.at[:, c0 - 256 : c0 + 256], PR.at[:, (n - 1) * 256 : (n + 1) * 256],
                ps_s.at[n // 2], ps_r.at[n // 2], peer,
            )
            c.start()
            pc.append(c)

    @pl.loop(0, 4)
    def _(i):
        finish(t * 4 + i)

    for n in range(8):
        dst = (XO1, XP1)[n // 4]
        c0 = (n % 4) * 256
        p = mm(AT[pl.ds(mine, 512), :], WO[:, n * 256 : (n + 1) * 256]).astype(bf16).astype(f32)
        if n % 2 == 0:
            with jax.named_scope(f"w_p{n}"):
                pc[n // 2].wait_recv()
        dst[:, c0 : c0 + 256] = (p + PR[:, n * 256 : (n + 1) * 256].astype(f32)).astype(bf16)
        if n % 2 == 1:
            c = pltpu.make_async_copy(
                dst.at[:, c0 - 256 : c0 + 256], out.at[:, (n - 1) * 256 : (n + 1) * 256], osem.at[n // 2]
            )
            c.start()
            oc.append(c)

    with jax.named_scope("w_snd"):
        for c in xc + sends + pc:
            c.wait_send()

        @pl.loop(1, nsp)
        def _(j):
            k = lax.rem(me + j, nsp)
            remote(FS, FR.at[me], fs_s.at[k], fs_r.at[me], {"sp": k}).wait_send()
            remote(SS.at[k], SR.at[me], ss_s.at[k], ss_r.at[me], {"sp": k}).wait_send()
            remote(ES.at[k], ER.at[me], es_s.at[k], es_r.at[me], {"sp": k}).wait_send()

        for c in oc:
            c.wait()


def tables(blocks):
    freq = 10000.0 ** (-(np.arange(128) % 32) / 32.0)
    a = np.arange(blocks)[:, None] * 128.0 * freq[None, :]
    r = np.arange(128)[:, None] * freq[None, :]
    return (
        np.stack([np.cos(a), np.sin(a)]).astype(np.float32),
        np.stack([np.cos(r), np.sin(r)]).astype(np.float32),
    )


def local(
    nsp, inputs, mix_gain, w_query, w_key, w_value, query_gain, key_gain, sink_logit, w_inner, w_bmat, w_cmat,
    w_gate, w_step, conv_inner, conv_bmat, conv_cmat, step_bias, decay_rate, decay_offset, start_state,
    group_gain, w_out_attn, w_out_state,
):
    wst = jnp.transpose(w_step, (1, 2, 0)).reshape(16, D)
    off = jnp.transpose(decay_offset, (1, 2, 0)).reshape(16, TOK)
    tabs, rows = tables(nsp * NB)
    hbm = pl.BlockSpec(memory_space=pl.ANY)
    vm = pl.BlockSpec(memory_space=pltpu.VMEM)
    sm = pl.BlockSpec(memory_space=pltpu.SMEM)
    V = pltpu.VMEM
    dma = pltpu.SemaphoreType.DMA
    return pl.pallas_call(
        lambda *refs: kernel(nsp, *refs),
        name="layer",
        out_shape=jax.ShapeDtypeStruct((TOK // 2, D), bf16),
        in_specs=[hbm, vm, hbm, hbm, hbm, hbm, hbm, hbm, hbm, vm, vm, vm, sm, vm, vm, vm, sm, sm, vm, hbm, vm, hbm, hbm, hbm, hbm],
        out_specs=hbm,
        scratch_shapes=[
            V((512, HALF), bf16), V((512, HALF), bf16), V((512, HALF), bf16), V((512, HALF), bf16),
            V((2, 512, 128), f32),
            V((D, 512), bf16), V((D, 256), bf16), V((D, 512), bf16), V((D, 512), bf16), V((D, 512), bf16),
            V((1024, D), bf16), V((128, D), bf16),
            V((2, NB, 512, 128), bf16), V((2, TOK + 256, 128), bf16), V((2, TOK + 256, 256), bf16),
            V((2, 128, 256), bf16), V((2, 128, 256), bf16),
            V((8, TOK + 16, 128), f32), V((2, 8, 8, 128), f32), V((TOK, 512), f32), V((8, 1024), f32),
            V((TOK, 128), f32), V((TOK, 128), f32),
            V((NB, 16, 128), f32), V((NB, 16, 128), f32), V((TOK, 128), f32),
            V((TOK, 512), bf16), V((TOK, 256), bf16), V((TOK, 256), bf16),
            V((TOK, 1024), f32), V((NB, 8, 1024), f32), V((NB, 128, 1024), f32),
            V((nsp, 16, 512), bf16), V((nsp, 16, 512), bf16), V((8, 128), f32), V((nsp, 8, 128), f32),
            V((nsp, 16, 512), bf16), V((nsp, 16, 512), bf16), V((nsp, 8, 512), f32),
            V((NB, 128, 1024), bf16),
            V((TOK, 512), f32), V((TOK, 1024), bf16), V((512, D), bf16), V((2, 128, 512), f32), V((2, 256, 1024), bf16),
            V((256, 256), bf16), V((2, 512, 128), f32), V((2, 8, 128), f32), V((2, 128, 128), f32),
            dma((5,)), dma((14,)), dma((2,)), dma((2,)), dma((2,)), dma((2,)), dma((2,)), dma((2,)),
            dma((nsp,)), dma((nsp,)), dma((nsp,)), dma((nsp,)), dma((nsp,)), dma((nsp,)), dma((4,)), dma((4,)), dma((4,)),
        ],
        compiler_params=pltpu.CompilerParams(
            collective_id=0, has_side_effects=True, vmem_limit_bytes=56 * 1024 * 1024
        ),
    )(
        inputs, mix_gain.reshape(1, D), w_query, w_key, w_value, w_inner, w_bmat, w_cmat, w_gate, wst,
        query_gain.reshape(1, 64), key_gain.reshape(1, 64), sink_logit, conv_inner, conv_bmat, conv_cmat,
        step_bias, decay_rate, off, start_state.reshape(2, 512, 128),
        group_gain.reshape(1, 512), w_out_attn, w_out_state, jnp.asarray(tabs), jnp.asarray(rows),
    )


def solution(mesh):
    nsp = mesh.shape["sp"]
    return jax.shard_map(
        lambda *args: local(nsp, *args),
        mesh=mesh,
        in_specs=(
            P(("fs", "sp"), "tp"), P(), P(None, "tp"), P(None, "tp"), P(None, "tp"), P(), P(), P("tp"),
            P(None, "tp"), P(None, "tp"), P(None, "tp"), P(None, "tp"), P(None, None, "tp"),
            P(None, "tp"), P(None, "tp"), P(None, "tp"), P(None, "tp"), P(None, "tp"),
            P("sp", None, "tp"), P("fs", "tp", None, None), P("tp"), P("tp", None), P("tp", None),
        ),
        out_specs=P(("fs", "sp", "tp"), None),
        check_vma=False,
    )
```

time: 81.9 us -> 60.3 us (0.74)
  Pallas kernels: 70.7 us -> 56.7 us
  local copies, waits for them, and re-layouts: 8.68 us -> 3.16 us
  other arithmetic: 2.14 us -> 0 us
    pallas_call x1, Pallas kernels: 70.7 us -> 56.7 us  [local(): pl.pallas_call(lambda *refs: kernel(nsp, *refs), name='layer', out_shape=...]
    broadcast_in_dim x4 -> x0, local copies, waits for them, and re-layouts: 1.66 us -> none  [the longest x2 0.83 us: local(): jnp.broadcast_to(step_bias.reshape(16, 1), (16, 128))]
    concatenate x1 -> x0, other arithmetic: 1.48 us -> none  [local(): jnp.concatenate([off, jnp.broadcast_to(step_bias.reshape(16, 1), (16, 128...]
    another operation x3 -> x0, local copies, waits for them, and re-layouts: 1.25 us -> none  [the longest x2 1.24 us: local(): kgain = jnp.tile(key_gain, 2).reshape(1, 128)]
    reshape x1 -> x0, local copies, waits for them, and re-layouts: 1.11 us -> none  [local(): wst = jnp.pad(w_step.reshape(D, 16), ((0, 0), (0, 112)))]
    pad x1 -> x0, local copies, waits for them, and re-layouts: 0.9 us -> none  [local(): wst = jnp.pad(w_step.reshape(D, 16), ((0, 0), (0, 112)))]
where the time goes in v1:
time: 60.3 us; the launch traced here: 59.9 us
  Pallas kernels  56.7 us (94%)
  local copies, waits for them, and re-layouts  3.16 us (5%)
    pallas_call x1, Pallas kernels, local(): pl.pallas_call(lambda *refs: kernel(nsp, *refs), name='layer', out_shape=...  56.7 us
    unnamed x1, local copies, waits for them, and re-layouts  3.16 us

profile of v1, /device:TPU:1, one launch (start us, length us, event | category | flops | bytes accessed | tf_op | source)
XLA Modules:
  0.0 59.9 jit_solution(7282792632756029413)
XLA Ops:
  0.0 56.7 %layer.1 = bf16[512,2048]{1,0:T(8,128)(2,1)} custom-call(bf16[1024,1024]{1,0:T(8,128)(2,1)} %refs_0_.1, f32[1,2048]{1,0:T(1,128)} %bitcast.14, bf16[2048,512]{1,0:T(8,128)(2,1)} %refs_2_.1, bf16[2048,128]{1,0:T(8,128)(2,1)} %refs_3_.1, bf16[2048,128]{1,0:T(8,128)(2,1)} %refs_4_.1, bf16[2048,512]{1,0:T(8,128)(2,1)} %refs_5_.1, bf16[2048,256]{1,0:T(8,128)(2,1)} %refs_6_.1, ...), custom_call_target="tpu_custom_call" | custom-call | tf_op jit(solution)/shard_map/layer/pallas_call | solution.py:571
  56.7 3.2 %copy.27 = bf16[512,2048]{1,0:T(8,128)(2,1)} copy(bf16[512,2048]{1,0:T(8,128)(2,1)} %layer.1) | data formatting | bytes 4194304

commit v2 on v1

--- a/solution.py
+++ b/solution.py
@@ -37,13 +37,14 @@
 
 def kernel(
     nsp,
-    x, gain, wq, wk, wv, wi, wb, wc, wg, wst, qgain, kgain, sink, ci, cb, cc,
-    bias, rate, off, start, ggain, woa, wos, tabs, rows,
+    x, gain_, wq, wk, wv, wi, wb, wc, wg, wst_, qgain_, kgain_, sink_, ci_, cb_, cc_,
+    bias_, rate_, off_, start, ggain_, woa, wos, tabs, rows,
     out,
     XO0, XO1, XP0, XP1, RS, WQ, WKV, WI, WBC, WG, WO, WST, QM, KD, VD, KVS, KVR, MX, MXR, SG, TAPS,
     COS, SIN, STP, CUM, MT, INN, BA, CA, E1X, FL, BS, SS, SR, FS, FR, ES, ER, EF, ENT,
     WN, AT, PR, SST, SPR, HM, STV, TBV, RWV,
-    lsem, wsem, xs_s, xs_r, hs_s, hs_r, ms_s, ms_r, ss_s, ss_r, fs_s, fs_r, es_s, es_r, ps_s, ps_r, osem,
+    gain, wst, qgain, kgain, sink, ci, cb, cc, bias, rate, off, ggain,
+    asem, lsem, wsem, xs_s, xs_r, hs_s, hs_r, ms_s, ms_r, ss_s, ss_r, fs_s, fs_r, es_s, es_r, ps_s, ps_r,
 ):
     me = lax.axis_index("sp")
     t = lax.axis_index("tp")
@@ -87,7 +88,16 @@
         pltpu.make_async_copy(woa, WO.at[0:512], wsem.at[12]),
         pltpu.make_async_copy(wos, WO.at[512:1024], wsem.at[13]),
     ]
-    for c in [xl[0]] + first + [xl[1]] + small + second + third:
+    args = [
+        pltpu.make_async_copy(a, b, asem.at[i])
+        for i, (a, b) in enumerate(
+            [
+                (gain_, gain), (wst_, wst), (qgain_, qgain), (kgain_, kgain), (sink_, sink), (ci_, ci), (cb_, cb),
+                (cc_, cc), (bias_, bias), (rate_, rate), (off_, off), (ggain_, ggain),
+            ]
+        )
+    ]
+    for c in [args[0], xl[0], args[1]] + first[:2] + args[2:]:
         c.start()
 
     lane = iota((1, 128), 1)
@@ -97,15 +107,9 @@
     ones_lanes = jnp.ones((128, 128), bf16)
     HM[...] = jnp.where(iota((256, 256), 0) // 64 == iota((256, 256), 1) // 64, 1.0 / 64, 0.0).astype(bf16)
     WST[...] = jnp.zeros((128, D), bf16)
-    WST[0:16, :] = wst[...]
-    TAPS[0:5, 0:512] = ci[...].astype(f32)
-    TAPS[0:5, 512:768] = cb[...].astype(f32)
-    TAPS[0:5, 768:1024] = cc[...].astype(f32)
-    qg = jnp.concatenate([qgain[...], qgain[...]], axis=1) * (LOG2E / 8.0)
-    kg = jnp.concatenate([kgain[...], kgain[...]], axis=1)
-
-    def scale(ref, off_, h, begin):
-        g = gain[0:1, pl.ds(off_, HALF)]
+
+    def scale(ref, at, h, begin):
+        g = gain[0:1, pl.ds(at, HALF)]
         for i in range(8):
             r = i * 64
             v = ref[r : r + 64, :].astype(f32)
@@ -116,6 +120,8 @@
             else:
                 RS[h, r : r + 64, :] = lax.rsqrt((RS[h, r : r + 64, :] + ss) * (1.0 / D) + EPS)
 
+    for c in first[2:] + [xl[1]] + small:
+        c.start()
     mixed_tiles = [(WI, 0), (WI, 256), (WBC, 0), (WBC, 256)]
 
     def part_one(h):
@@ -129,11 +135,17 @@
         for n, (w, c0) in enumerate(mixed_tiles):
             E1X[rows_, n * 256 : (n + 1) * 256] = mm(xs, w[pl.ds(own, HALF), c0 : c0 + 256])
 
-    xl[0].wait()
+    with jax.named_scope("w_xl0"):
+        xl[0].wait()
+        for c in args[:2]:
+            c.wait()
+    WST[0:16, :] = wst[...]
+    for c in second + third:
+        c.start()
     scale(XO[0], own, 0, True)
-    first[0].wait()
-    first[1].wait()
-    part_one(0)
+    with jax.named_scope("w_f0"):
+        first[0].wait()
+        first[1].wait()
     with jax.named_scope("w_barrier"):
         pl.semaphore_wait(barrier, nsp)
     xc = []
@@ -141,12 +153,19 @@
         c = remote(x.at[h * 512 : (h + 1) * 512, :], XP[h], xs_s.at[h], xs_r.at[h], peer)
         c.start()
         xc.append(c)
-    xl[1].wait()
+    part_one(0)
+    with jax.named_scope("w_xl1"):
+        xl[1].wait()
+        for c in small + args[2:]:
+            c.wait()
+    TAPS[0:5, 0:512] = ci[...].astype(f32)
+    TAPS[0:5, 512:768] = cb[...].astype(f32)
+    TAPS[0:5, 768:1024] = cc[...].astype(f32)
+    qg = jnp.concatenate([qgain[...], qgain[...]], axis=1) * (LOG2E / 8.0)
+    kg = jnp.concatenate([kgain[...], kgain[...]], axis=1)
     scale(XO[1], own, 1, True)
     part_one(1)
 
-    for c in small:
-        c.wait()
     for d in range(2):
         for q in range(4):
             SST[d, :, q * 128 : (q + 1) * 128] = STV[d, q * 128 : (q + 1) * 128, :].T
@@ -213,20 +232,6 @@
         c.start()
         sends.append(c)
 
-    for h in range(2):
-        with jax.named_scope(f"w_x{h}"):
-            xc[h].wait_recv()
-        if h == 0:
-            with jax.named_scope("w_w2"):
-                for c in second:
-                    c.wait()
-        scale(XP[h], oth, h, False)
-        part_two(h)
-
-    with jax.named_scope("w_qg"):
-        third[0].wait()
-        third[1].wait()
-
     row16 = iota((16, 128), 0)
     bias_c = jnp.zeros((16, 128), f32)
     rate_c = jnp.zeros((16, 128), f32)
@@ -255,10 +260,6 @@
 
     def pre_block(b):
         r0 = b * BLK
-        m = MT[r0 : r0 + 128, :]
-        hi = m.astype(bf16)
-        lo = (m - hi.astype(f32)).astype(bf16)
-        both = jnp.concatenate([hi, lo], axis=1)
         bts = [None, None]
         for ct in (4, 5, 6, 7, 0, 1, 2, 3):
             acc = None
@@ -278,27 +279,39 @@
                 g = ct // 2
                 for d in range(2):
                     c0 = d * 512 + g * 256
-                    e2x = mm(both, SPR[1, :, c0 : c0 + 256])
-                    loaded = (INN[r0 : r0 + 128, g * 256 : (g + 1) * 256].astype(f32) * e2x).astype(bf16)
+                    loaded = (
+                        INN[r0 : r0 + 128, g * 256 : (g + 1) * 256].astype(f32) * BS[b, :, c0 : c0 + 256]
+                    ).astype(bf16)
                     BS[b, :, c0 : c0 + 256] = mm(bts[g], loaded)
-        e1x = mm(both, SPR[0])
-        E1X[r0 : r0 + 128, :] = e1x
-        FL[b, 0:1, 0:512] = e1x[127:128, 0:512]
-        FL[b, 0:1, 512:1024] = e1x[0:1, 512:1024]
-
-    def query_tile(h, n):
+
+    def spread(h):
+        m = MT[h * 512 : (h + 1) * 512, :]
+        hi = m.astype(bf16)
+        lo = (m - hi.astype(f32)).astype(bf16)
+        both = jnp.concatenate([hi, lo], axis=1)
+        for n in range(4):
+            c = slice(n * 256, (n + 1) * 256)
+            e1x = mm(both, SPR[0, :, c])
+            E1X[h * 512 : (h + 1) * 512, c] = e1x
+            e2x = mm(both, SPR[1, :, c])
+            for i in range(4):
+                r = i * 128 + (127 if n < 2 else 0)
+                FL[h * 4 + i, 0:1, c] = e1x[r : r + 1, :]
+                BS[h * 4 + i, :, c] = e2x[i * 128 : (i + 1) * 128]
+
+    def query(h):
         h0 = h * 512
-        p = mm(XO[h][...], WQ[pl.ds(own, HALF), n * 256 : (n + 1) * 256]) + mm(
-            XP[h][...], WQ[pl.ds(oth, HALF), n * 256 : (n + 1) * 256]
-        )
-        qp = [(p[:, q * 128 : (q + 1) * 128] * RS[h]).astype(bf16).astype(f32) for q in range(2)]
-        ms = mm(jnp.concatenate([(v * v).astype(bf16) for v in qp], axis=1), HM[...])
-        for q in range(2):
-            for i in range(4):
-                sub = slice(i * 128, (i + 1) * 128)
-                v = rotated(qp[q][sub] * lax.rsqrt(ms[sub, q * 128 : (q + 1) * 128] + EPS) * qg, h0 + i * 128)
-                QM[n, h * 4 + i, q * 256 : q * 256 + 128, :] = jnp.where(lo_half, v, 0.0).astype(bf16)
-                QM[n, h * 4 + i, q * 256 + 128 : q * 256 + 256, :] = jnp.where(lo_half, 0.0, v).astype(bf16)
+        p = mm(XO[h][...], WQ[pl.ds(own, HALF), :]) + mm(XP[h][...], WQ[pl.ds(oth, HALF), :])
+        qp = [(p[:, q * 128 : (q + 1) * 128] * RS[h]).astype(bf16).astype(f32) for q in range(4)]
+        for n in range(2):
+            ms = mm(jnp.concatenate([(v * v).astype(bf16) for v in qp[2 * n : 2 * n + 2]], axis=1), HM[...])
+            for q in range(2):
+                for i in range(4):
+                    sub = slice(i * 128, (i + 1) * 128)
+                    v = qp[2 * n + q][sub] * lax.rsqrt(ms[sub, q * 128 : (q + 1) * 128] + EPS) * qg
+                    v = rotated(v, h0 + i * 128)
+                    QM[n, h * 4 + i, q * 256 : q * 256 + 128, :] = jnp.where(lo_half, v, 0.0).astype(bf16)
+                    QM[n, h * 4 + i, q * 256 + 128 : q * 256 + 256, :] = jnp.where(lo_half, 0.0, v).astype(bf16)
 
     def gate_tile(h, n):
         h0 = h * 512
@@ -309,16 +322,36 @@
             gp = (p[:, q * 128 : (q + 1) * 128] * RS[h]).astype(bf16).astype(f32)
             SG[h0 : h0 + 512, n * 256 + q * 128 : n * 256 + (q + 1) * 128] = silu(gp)
 
-    for b in range(NB):
+    with jax.named_scope("w_x0"):
+        xc[0].wait_recv()
+        for c in second:
+            c.wait()
+    scale(XP[0], oth, 0, False)
+    part_two(0)
+    with jax.named_scope("w_x1"):
+        xc[1].wait_recv()
+        third[0].wait()
+        third[1].wait()
+    scale(XP[1], oth, 1, False)
+    part_two(1)
+    for b in range(4):
         steps(b)
-    for i, b in enumerate((1, 2, 3, 4, 5, 6, 7, 0)):
-        if i == 6:
-            with jax.named_scope("w_halo"):
-                for e in range(2):
-                    remote(MX.at[:, 8:16, :], MXR.at[e], ms_s.at[e], ms_r.at[e], left).wait_recv()
-            MX[:, 0:8, :] = jnp.where(me == 0, 0.0, MXR[0])
-            MX[:, 8 + TOK : 16 + TOK, :] = jnp.where(me == nsp - 1, 0.0, MXR[1])
-        (query_tile if i < 4 else gate_tile)((i // 2) % 2, i % 2)
+    spread(0)
+    query(0)
+    for b in (1, 2):
+        pre_block(b)
+    for b in range(4, 8):
+        steps(b)
+    spread(1)
+    query(1)
+    for b in (3, 4, 5, 6):
+        pre_block(b)
+    with jax.named_scope("w_halo"):
+        for e in range(2):
+            remote(MX.at[:, 8:16, :], MXR.at[e], ms_s.at[e], ms_r.at[e], left).wait_recv()
+    MX[:, 0:8, :] = jnp.where(me == 0, 0.0, MXR[0])
+    MX[:, 8 + TOK : 16 + TOK, :] = jnp.where(me == nsp - 1, 0.0, MXR[1])
+    for b in (7, 0):
         pre_block(b)
 
     fd = FL[0, 0:1, :]
@@ -349,6 +382,8 @@
     with jax.named_scope("w_kvh"):
         for e in range(2):
             remote(KVS.at[e], KVR.at[e], hs_s.at[e], hs_r.at[e], left).wait_recv()
+        for c in sends:
+            c.wait_send()
     for e in range(2):
         keep_kv(
             KVR[e, :, 0:128].astype(f32), KVR[e, :, 128:256].astype(f32), 0 if e == 0 else 128 + TOK
@@ -360,35 +395,42 @@
         off_r = jnp.where((me == nsp - 1) & (b == NB - 1), 1024, 0)
         keep_l = g_col >= g_row + off_l
         keep_r = g_col <= g_row - off_r
+        low, high = [], []
+        for z in range(2):
+            row, col = iota((64, 128), 0) + z * 64, iota((64, 128), 1)
+            low.append(col >= row + off_l)
+            high.append(col <= row - off_r)
         for g in range(2):
-            kk = KD[g, pl.ds(r0, 384), :]
-            vv = VD[g, pl.ds(r0, 384), :]
-            s = lax.dot_general(QM[g, b], kk, NT, preferred_element_type=f32)
-            ps, ms = [], []
+            s = lax.dot_general(QM[g, b], KD[g, pl.ds(r0, 384), :], NT, preferred_element_type=f32)
+            for kt in range(3):
+                MX[g * 3 + kt, 0:512, :] = s[:, kt * 128 : (kt + 1) * 128]
+        for g in range(2):
             for j in range(4):
-                sj = s[j * 128 : (j + 1) * 128]
-                sl = jnp.where(keep_l, sj[:, 0:128], NEG)
-                sm = sj[:, 128:256]
-                sr = jnp.where(keep_r, sj[:, 256:384], NEG)
                 sk = sink[g * 4 + j] * LOG2E
-                m = jnp.max(jnp.maximum(jnp.maximum(sl, sm), sr), axis=1, keepdims=True)
-                m = jnp.broadcast_to(jnp.maximum(m, sk), (128, 128))
-                ps.append(jnp.concatenate([jnp.exp2(v - m).astype(bf16) for v in (sl, sm, sr)], axis=1))
-                ms.append(jnp.exp2(sk - m))
-            o = mm(jnp.concatenate(ps, axis=0), vv)
-            res = [
-                o[j * 128 : (j + 1) * 128, 0:128] / (o[j * 128 : (j + 1) * 128, 128:256] + ms[j]) for j in range(4)
-            ]
+                for z in range(2):
+                    r = j * 128 + z * 64
+                    sl = jnp.where(low[z], MX[g * 3, r : r + 64, :], NEG)
+                    sm = MX[g * 3 + 1, r : r + 64, :]
+                    sr = jnp.where(high[z], MX[g * 3 + 2, r : r + 64, :], NEG)
+                    m = jnp.max(jnp.maximum(jnp.maximum(sl, sm), sr), axis=1, keepdims=True)
+                    m = jnp.broadcast_to(jnp.maximum(m, sk), (64, 128))
+                    WI[g * 512 + r : g * 512 + r + 64, 0:128] = jnp.exp2(sl - m).astype(bf16)
+                    WI[g * 512 + r : g * 512 + r + 64, 128:256] = jnp.exp2(sm - m).astype(bf16)
+                    WI[g * 512 + r : g * 512 + r + 64, 256:384] = jnp.exp2(sr - m).astype(bf16)
+                    COS[g * 512 + r : g * 512 + r + 64, :] = jnp.exp2(sk - m)
+            o = mm(WI[g * 512 : (g + 1) * 512, 0:384], VD[g, pl.ds(r0, 384), :])
             for pair in range(2):
+                res = []
+                for j in (2 * pair, 2 * pair + 1):
+                    sub = slice(j * 128, (j + 1) * 128)
+                    res.append(o[sub, 0:128] / (o[sub, 128:256] + COS[g * 512 + j * 128 : g * 512 + (j + 1) * 128, :]))
                 tile = g * 2 + pair
                 AT[pl.ds(r0, 128), tile * 128 : (tile + 1) * 128] = jnp.where(
-                    lo_half, res[2 * pair], res[2 * pair + 1]
+                    lo_half, res[0], res[1]
                 ).astype(bf16)
 
     def inside(b):
         r0 = pl.multiple_of(b * BLK, BLK)
-        lower = g_row >= g_col
-        diag = g_row == g_col
         for g in range(2):
             cm = CA[pl.ds(r0, 128), g * 128 : (g + 1) * 128]
             bm = BA[pl.ds(r0, 128), g * 128 : (g + 1) * 128]
@@ -396,23 +438,26 @@
             for pair in range(2):
                 tile = g * 2 + pair
                 xt = INN[pl.ds(r0, 128), tile * 128 : (tile + 1) * 128].astype(f32)
-                ws = []
                 for j in range(2):
                     h = tile * 2 + j
-                    dif = jnp.where(
-                        lower,
-                        MT[pl.ds(r0, 128), h : h + 1] - CUM[b, h : h + 1, :],
-                        MT[pl.ds(r0, 128), 8 + h : 9 + h] - CUM[b, 8 + h : 9 + h, :],
-                    )
-                    sf, sb = STP[b, h : h + 1, :], STP[b, 8 + h : 9 + h, :]
-                    st = jnp.where(diag, sf + sb, jnp.where(lower, sf, sb))
-                    ws.append((sc * jnp.exp2(dif) * st).astype(bf16))
-                both = jnp.concatenate(ws, axis=1)
+                    for z in range(2):
+                        row, col = iota((64, 128), 0) + z * 64, iota((64, 128), 1)
+                        rz = pl.multiple_of(r0 + z * 64, 64)
+                        dif = jnp.where(
+                            row >= col,
+                            MT[pl.ds(rz, 64), h : h + 1] - CUM[b, h : h + 1, :],
+                            MT[pl.ds(rz, 64), 8 + h : 9 + h] - CUM[b, 8 + h : 9 + h, :],
+                        )
+                        sf, sb = STP[b, h : h + 1, :], STP[b, 8 + h : 9 + h, :]
+                        st = jnp.where(row == col, sf + sb, jnp.where(row >= col, sf, sb))
+                        WBC[tile * 128 + z * 64 : tile * 128 + z * 64 + 64, j * 128 : (j + 1) * 128] = (
+                            sc[z * 64 : z * 64 + 64] * jnp.exp2(dif) * st
+                        ).astype(bf16)
                 xx = jnp.concatenate(
                     [jnp.where(lo_half, xt, 0.0).astype(bf16), jnp.where(lo_half, 0.0, xt).astype(bf16)],
                     axis=0,
                 )
-                WN[pl.ds(r0, 128), tile * 128 : (tile + 1) * 128] = mm(both, xx)
+                WN[pl.ds(r0, 128), tile * 128 : (tile + 1) * 128] = mm(WBC[tile * 128 : (tile + 1) * 128, 0:256], xx)
 
     @pl.loop(0, 5)
     def _(b):
@@ -449,6 +494,11 @@
     def _(b):
         attend(b)
         inside(b)
+
+    with jax.named_scope("c_gate"):
+        for h in range(2):
+            for n in range(2):
+                gate_tile(h, n)
 
     with jax.named_scope("w_e"):
         for j in range(1, nsp):
@@ -471,21 +521,26 @@
 
     group_mean = jnp.full((256, 256), 1.0 / 256, bf16)
 
-    def finish(b):
-        r0 = pl.multiple_of(b * BLK, BLK)
+    def finish(b0):
         for g in range(2):
-            cm = CA[pl.ds(r0, 128), g * 128 : (g + 1) * 128]
             c0, c1 = g * 256, (g + 1) * 256
-            tot = (
-                WN[pl.ds(r0, 128), c0:c1]
-                + mm(cm, ENT[b, :, c0:c1]) * E1X[pl.ds(r0, 128), c0:c1]
-                + mm(cm, ENT[b, :, 512 + c0 : 512 + c1]) * E1X[pl.ds(r0, 128), 512 + c0 : 512 + c1]
-            )
-            gated = tot * SG[pl.ds(r0, 128), c0:c1]
-            ms = mm((gated * gated).astype(bf16), group_mean)
-            AT[pl.ds(r0, 128), 512 + c0 : 512 + c1] = (
-                gated * lax.rsqrt(ms + EPS) * ggain[0:1, c0:c1]
-            ).astype(bf16)
+            gated = []
+            for i in range(4):
+                b = b0 + i
+                r0 = pl.multiple_of(b * BLK, BLK)
+                cm = CA[pl.ds(r0, 128), g * 128 : (g + 1) * 128]
+                tot = (
+                    WN[pl.ds(r0, 128), c0:c1]
+                    + mm(cm, ENT[b, :, c0:c1]) * E1X[pl.ds(r0, 128), c0:c1]
+                    + mm(cm, ENT[b, :, 512 + c0 : 512 + c1]) * E1X[pl.ds(r0, 128), 512 + c0 : 512 + c1]
+                )
+                gated.append(tot * SG[pl.ds(r0, 128), c0:c1])
+            ms = mm(jnp.concatenate([(v * v).astype(bf16) for v in gated], axis=0), group_mean)
+            for i in range(4):
+                r0 = pl.multiple_of((b0 + i) * BLK, BLK)
+                AT[pl.ds(r0, 128), 512 + c0 : 512 + c1] = (
+                    gated[i] * lax.rsqrt(ms[i * 128 : (i + 1) * 128] + EPS) * ggain[0:1, c0:c1]
+                ).astype(bf16)
 
     with jax.named_scope("w_wo"):
         third[2].wait()
@@ -493,45 +548,45 @@
     other = pl.multiple_of((1 - t) * 512, 512)
     mine = pl.multiple_of(t * 512, 512)
     pc = []
-    oc = []
-
-    @pl.loop(0, 4)
-    def _(i):
-        finish((1 - t) * 4 + i)
-
-    for n in range(8):
-        dst = (XO0, XP0)[n // 4]
-        c0 = (n % 4) * 256
-        dst[:, c0 : c0 + 256] = mm(AT[pl.ds(other, 512), :], WO[:, n * 256 : (n + 1) * 256]).astype(bf16)
-        if n % 2 == 1:
-            c = remote(
-                dst.at[:, c0 - 256 : c0 + 256], PR.at[:, (n - 1) * 256 : (n + 1) * 256],
-                ps_s.at[n // 2], ps_r.at[n // 2], peer,
-            )
-            c.start()
-            pc.append(c)
-
-    @pl.loop(0, 4)
-    def _(i):
-        finish(t * 4 + i)
-
-    for n in range(8):
+
+    with jax.named_scope("c_fin0"):
+        finish((1 - t) * 4)
+
+    for n in range(4):
+        dst = (XO0, XP0)[n // 2].at[:, (n % 2) * 512 : (n % 2) * 512 + 512]
+        cols = slice(n * 512, (n + 1) * 512)
+        dst[...] = mm(AT[pl.ds(other, 512), :], WO[:, cols]).astype(bf16)
+        c = remote(dst, PR.at[:, cols], ps_s.at[n], ps_r.at[n], peer)
+        c.start()
+        pc.append(c)
+
+    with jax.named_scope("c_fin1"):
+        finish(t * 4)
+
+    def own_tile(n):
         dst = (XO1, XP1)[n // 4]
         c0 = (n % 4) * 256
-        p = mm(AT[pl.ds(mine, 512), :], WO[:, n * 256 : (n + 1) * 256]).astype(bf16).astype(f32)
-        if n % 2 == 0:
-            with jax.named_scope(f"w_p{n}"):
-                pc[n // 2].wait_recv()
-        dst[:, c0 : c0 + 256] = (p + PR[:, n * 256 : (n + 1) * 256].astype(f32)).astype(bf16)
-        if n % 2 == 1:
-            c = pltpu.make_async_copy(
-                dst.at[:, c0 - 256 : c0 + 256], out.at[:, (n - 1) * 256 : (n + 1) * 256], osem.at[n // 2]
-            )
-            c.start()
-            oc.append(c)
+        dst[:, c0 : c0 + 256] = mm(AT[pl.ds(mine, 512), :], WO[:, n * 256 : (n + 1) * 256]).astype(bf16)
+
+    def sum_tile(n):
+        own_part = (XO1, XP1)[n // 4][:, (n % 4) * 256 : (n % 4) * 256 + 256].astype(f32)
+        out[:, n * 256 : (n + 1) * 256] = (own_part + PR[:, n * 256 : (n + 1) * 256].astype(f32)).astype(bf16)
+
+    with jax.named_scope("c_out1"):
+        for n in range(3):
+            own_tile(n)
+    with jax.named_scope("w_p"):
+        for c in pc:
+            c.wait_recv()
+    with jax.named_scope("c_out2"):
+        for n in range(3, 8):
+            p = mm(AT[pl.ds(mine, 512), :], WO[:, n * 256 : (n + 1) * 256]).astype(bf16).astype(f32)
+            out[:, n * 256 : (n + 1) * 256] = (p + PR[:, n * 256 : (n + 1) * 256].astype(f32)).astype(bf16)
+            if n < 6:
+                sum_tile(n - 3)
 
     with jax.named_scope("w_snd"):
-        for c in xc + sends + pc:
+        for c in xc + pc:
             c.wait_send()
 
         @pl.loop(1, nsp)
@@ -540,9 +595,6 @@
             remote(FS, FR.at[me], fs_s.at[k], fs_r.at[me], {"sp": k}).wait_send()
             remote(SS.at[k], SR.at[me], ss_s.at[k], ss_r.at[me], {"sp": k}).wait_send()
             remote(ES.at[k], ER.at[me], es_s.at[k], es_r.at[me], {"sp": k}).wait_send()
-
-        for c in oc:
-            c.wait()
 
 
 def tables(blocks):
@@ -565,15 +617,14 @@
     tabs, rows = tables(nsp * NB)
     hbm = pl.BlockSpec(memory_space=pl.ANY)
     vm = pl.BlockSpec(memory_space=pltpu.VMEM)
-    sm = pl.BlockSpec(memory_space=pltpu.SMEM)
     V = pltpu.VMEM
     dma = pltpu.SemaphoreType.DMA
     return pl.pallas_call(
         lambda *refs: kernel(nsp, *refs),
         name="layer",
-        out_shape=jax.ShapeDtypeStruct((TOK // 2, D), bf16),
-        in_specs=[hbm, vm, hbm, hbm, hbm, hbm, hbm, hbm, hbm, vm, vm, vm, sm, vm, vm, vm, sm, sm, vm, hbm, vm, hbm, hbm, hbm, hbm],
-        out_specs=hbm,
+        out_shape=pltpu.VMEM((TOK // 2, D), bf16),
+        in_specs=[hbm] * 25,
+        out_specs=vm,
         scratch_shapes=[
             V((512, HALF), bf16), V((512, HALF), bf16), V((512, HALF), bf16), V((512, HALF), bf16),
             V((2, 512, 128), f32),
@@ -591,8 +642,11 @@
             V((NB, 128, 1024), bf16),
             V((TOK, 512), f32), V((TOK, 1024), bf16), V((512, D), bf16), V((2, 128, 512), f32), V((2, 256, 1024), bf16),
             V((256, 256), bf16), V((2, 512, 128), f32), V((2, 8, 128), f32), V((2, 128, 128), f32),
-            dma((5,)), dma((14,)), dma((2,)), dma((2,)), dma((2,)), dma((2,)), dma((2,)), dma((2,)),
-            dma((nsp,)), dma((nsp,)), dma((nsp,)), dma((nsp,)), dma((nsp,)), dma((nsp,)), dma((4,)), dma((4,)), dma((4,)),
+            V((1, D), f32), V((16, D), bf16), V((1, 64), f32), V((1, 64), f32), pltpu.SMEM((8,), f32),
+            V((5, 512), bf16), V((5, 256), bf16), V((5, 256), bf16), pltpu.SMEM((2, 8), f32), pltpu.SMEM((2, 8), f32),
+            V((16, TOK), f32), V((1, 512), f32),
+            dma((12,)), dma((5,)), dma((14,)), dma((2,)), dma((2,)), dma((2,)), dma((2,)), dma((2,)), dma((2,)),
+            dma((nsp,)), dma((nsp,)), dma((nsp,)), dma((nsp,)), dma((nsp,)), dma((nsp,)), dma((4,)), dma((4,)),
         ],
         compiler_params=pltpu.CompilerParams(
             collective_id=0, has_side_effects=True, vmem_limit_bytes=56 * 1024 * 1024

time: 60.3 us -> 47.2 us (0.78)
  Pallas kernels: 56.7 us -> 45.8 us
  local copies, waits for them, and re-layouts: 3.16 us -> 1.32 us
    pallas_call x1, Pallas kernels: 56.7 us -> 45.8 us  [local(): pl.pallas_call(lambda *refs: kernel(nsp, *refs), name='layer', out_shape=...]
    unnamed x1, local copies, waits for them, and re-layouts: 3.16 us -> 1.32 us
where the time goes in v2:
time: 47.2 us; the launch traced here: 47.1 us
  Pallas kernels  45.8 us (97%)
  local copies, waits for them, and re-layouts  1.32 us (3%)
    pallas_call x1, Pallas kernels, local(): pl.pallas_call(lambda *refs: kernel(nsp, *refs), name='layer', out_shape=...  45.8 us
    unnamed x1, local copies, waits for them, and re-layouts  1.32 us

profile of v2, /device:TPU:1, one launch (start us, length us, event | category | flops | bytes accessed | tf_op | source)
XLA Modules:
  0.0 47.1 jit_solution(15034189472653993232)
XLA Ops:
  0.0 45.8 %layer.1 = bf16[512,2048]{1,0:T(8,128)(2,1)S(1)} custom-call(bf16[1024,1024]{1,0:T(8,128)(2,1)} %refs_0_.1, f32[1,2048]{1,0:T(1,128)} %bitcast.14, bf16[2048,512]{1,0:T(8,128)(2,1)} %refs_2_.1, bf16[2048,128]{1,0:T(8,128)(2,1)} %refs_3_.1, bf16[2048,128]{1,0:T(8,128)(2,1)} %refs_4_.1, bf16[2048,512]{1,0:T(8,128)(2,1)} %refs_5_.1, bf16[2048,256]{1,0:T(8,128)(2,1)} %refs_6_.1, ...), custom_call_target="tpu_custom_call" | custom-call | tf_op jit(solution)/shard_map/layer/pallas_call | solution.py:622
  45.8 1.3 %copy.27 = bf16[512,2048]{1,0:T(8,128)(2,1)} copy(bf16[512,2048]{1,0:T(8,128)(2,1)S(1)} %layer.1) | data formatting | bytes 4194304

commit v3 on v2

--- a/solution.py
+++ b/solution.py
@@ -258,18 +258,24 @@
             [cum, e1, e2, jnp.zeros((80, 128), f32)], axis=0
         ).T
 
+    def conv(b, ct):
+        r0 = b * BLK
+        acc = None
+        for j in range(5):
+            term = MX[ct, r0 + 6 + j : r0 + 6 + j + 128, :] * TAPS[j : j + 1, ct * 128 : (ct + 1) * 128]
+            acc = term if acc is None else acc + term
+        return silu(acc).astype(bf16)
+
+    def cmat_block(b):
+        for ct in (6, 7):
+            CA[b * BLK : (b + 1) * BLK, (ct - 6) * 128 : (ct - 5) * 128] = conv(b, ct)
+
     def pre_block(b):
         r0 = b * BLK
         bts = [None, None]
-        for ct in (4, 5, 6, 7, 0, 1, 2, 3):
-            acc = None
-            for j in range(5):
-                term = MX[ct, r0 + 6 + j : r0 + 6 + j + 128, :] * TAPS[j : j + 1, ct * 128 : (ct + 1) * 128]
-                acc = term if acc is None else acc + term
-            act = silu(acc).astype(bf16)
-            if ct >= 6:
-                CA[r0 : r0 + 128, (ct - 6) * 128 : (ct - 5) * 128] = act
-            elif ct >= 4:
+        for ct in (4, 5, 0, 1, 2, 3):
+            act = conv(b, ct)
+            if ct >= 4:
                 BA[r0 : r0 + 128, (ct - 4) * 128 : (ct - 3) * 128] = act
                 bts[ct - 4] = act.astype(f32).T.astype(bf16)
             else:
@@ -313,14 +319,13 @@
                     QM[n, h * 4 + i, q * 256 : q * 256 + 128, :] = jnp.where(lo_half, v, 0.0).astype(bf16)
                     QM[n, h * 4 + i, q * 256 + 128 : q * 256 + 256, :] = jnp.where(lo_half, 0.0, v).astype(bf16)
 
-    def gate_tile(h, n):
-        h0 = h * 512
-        p = mm(XO[h][...], WG[pl.ds(own, HALF), n * 256 : (n + 1) * 256]) + mm(
-            XP[h][...], WG[pl.ds(oth, HALF), n * 256 : (n + 1) * 256]
-        )
-        for q in range(2):
-            gp = (p[:, q * 128 : (q + 1) * 128] * RS[h]).astype(bf16).astype(f32)
-            SG[h0 : h0 + 512, n * 256 + q * 128 : n * 256 + (q + 1) * 128] = silu(gp)
+    def gate_rows(h, i):
+        rr = pl.multiple_of(i * 256, 256)
+        part = pl.ds(rr, 256)
+        p = mm(XO[h][part, :], WG[pl.ds(own, HALF), :]) + mm(XP[h][part, :], WG[pl.ds(oth, HALF), :])
+        for q in range(4):
+            gp = (p[:, q * 128 : (q + 1) * 128] * RS[h, part, :]).astype(bf16).astype(f32)
+            SG[pl.ds(h * 512 + rr, 256), q * 128 : (q + 1) * 128] = silu(gp)
 
     with jax.named_scope("w_x0"):
         xc[0].wait_recv()
@@ -379,6 +384,8 @@
         remote(FS, FR.at[me], fs_s.at[k], fs_r.at[me], {"sp": k}).start()
         remote(SS.at[k], SR.at[me], ss_s.at[k], ss_r.at[me], {"sp": k}).start()
 
+    for b in range(NB):
+        cmat_block(b)
     with jax.named_scope("w_kvh"):
         for e in range(2):
             remote(KVS.at[e], KVR.at[e], hs_s.at[e], hs_r.at[e], left).wait_recv()
@@ -389,7 +396,8 @@
             KVR[e, :, 0:128].astype(f32), KVR[e, :, 128:256].astype(f32), 0 if e == 0 else 128 + TOK
         )
 
-    def attend(b):
+    def attend(b, u):
+        den = (COS, SIN)[u]
         r0 = pl.multiple_of(b * BLK, BLK)
         off_l = jnp.where((me == 0) & (b == 0), 1024, 0)
         off_r = jnp.where((me == nsp - 1) & (b == NB - 1), 1024, 0)
@@ -403,33 +411,33 @@
         for g in range(2):
             s = lax.dot_general(QM[g, b], KD[g, pl.ds(r0, 384), :], NT, preferred_element_type=f32)
             for kt in range(3):
-                MX[g * 3 + kt, 0:512, :] = s[:, kt * 128 : (kt + 1) * 128]
+                MX[g * 3 + kt, u * 512 : u * 512 + 512, :] = s[:, kt * 128 : (kt + 1) * 128]
         for g in range(2):
             for j in range(4):
                 sk = sink[g * 4 + j] * LOG2E
                 for z in range(2):
                     r = j * 128 + z * 64
-                    sl = jnp.where(low[z], MX[g * 3, r : r + 64, :], NEG)
-                    sm = MX[g * 3 + 1, r : r + 64, :]
-                    sr = jnp.where(high[z], MX[g * 3 + 2, r : r + 64, :], NEG)
+                    sl = jnp.where(low[z], MX[g * 3, u * 512 + r : u * 512 + r + 64, :], NEG)
+                    sm = MX[g * 3 + 1, u * 512 + r : u * 512 + r + 64, :]
+                    sr = jnp.where(high[z], MX[g * 3 + 2, u * 512 + r : u * 512 + r + 64, :], NEG)
                     m = jnp.max(jnp.maximum(jnp.maximum(sl, sm), sr), axis=1, keepdims=True)
                     m = jnp.broadcast_to(jnp.maximum(m, sk), (64, 128))
-                    WI[g * 512 + r : g * 512 + r + 64, 0:128] = jnp.exp2(sl - m).astype(bf16)
-                    WI[g * 512 + r : g * 512 + r + 64, 128:256] = jnp.exp2(sm - m).astype(bf16)
-                    WI[g * 512 + r : g * 512 + r + 64, 256:384] = jnp.exp2(sr - m).astype(bf16)
-                    COS[g * 512 + r : g * 512 + r + 64, :] = jnp.exp2(sk - m)
-            o = mm(WI[g * 512 : (g + 1) * 512, 0:384], VD[g, pl.ds(r0, 384), :])
+                    WI[u * 1024 + g * 512 + r : u * 1024 + g * 512 + r + 64, 0:128] = jnp.exp2(sl - m).astype(bf16)
+                    WI[u * 1024 + g * 512 + r : u * 1024 + g * 512 + r + 64, 128:256] = jnp.exp2(sm - m).astype(bf16)
+                    WI[u * 1024 + g * 512 + r : u * 1024 + g * 512 + r + 64, 256:384] = jnp.exp2(sr - m).astype(bf16)
+                    den[g * 512 + r : g * 512 + r + 64, :] = jnp.exp2(sk - m)
+            o = mm(WI[u * 1024 + g * 512 : u * 1024 + (g + 1) * 512, 0:384], VD[g, pl.ds(r0, 384), :])
             for pair in range(2):
                 res = []
                 for j in (2 * pair, 2 * pair + 1):
                     sub = slice(j * 128, (j + 1) * 128)
-                    res.append(o[sub, 0:128] / (o[sub, 128:256] + COS[g * 512 + j * 128 : g * 512 + (j + 1) * 128, :]))
+                    res.append(o[sub, 0:128] / (o[sub, 128:256] + den[g * 512 + j * 128 : g * 512 + (j + 1) * 128, :]))
                 tile = g * 2 + pair
                 AT[pl.ds(r0, 128), tile * 128 : (tile + 1) * 128] = jnp.where(
                     lo_half, res[0], res[1]
                 ).astype(bf16)
 
-    def inside(b):
+    def inside(b, u):
         r0 = pl.multiple_of(b * BLK, BLK)
         for g in range(2):
             cm = CA[pl.ds(r0, 128), g * 128 : (g + 1) * 128]
@@ -450,19 +458,25 @@
                         )
                         sf, sb = STP[b, h : h + 1, :], STP[b, 8 + h : 9 + h, :]
                         st = jnp.where(row == col, sf + sb, jnp.where(row >= col, sf, sb))
-                        WBC[tile * 128 + z * 64 : tile * 128 + z * 64 + 64, j * 128 : (j + 1) * 128] = (
+                        WBC[u * 512 + tile * 128 + z * 64 : u * 512 + tile * 128 + z * 64 + 64, j * 128 : (j + 1) * 128] = (
                             sc[z * 64 : z * 64 + 64] * jnp.exp2(dif) * st
                         ).astype(bf16)
                 xx = jnp.concatenate(
                     [jnp.where(lo_half, xt, 0.0).astype(bf16), jnp.where(lo_half, 0.0, xt).astype(bf16)],
                     axis=0,
                 )
-                WN[pl.ds(r0, 128), tile * 128 : (tile + 1) * 128] = mm(WBC[tile * 128 : (tile + 1) * 128, 0:256], xx)
-
-    @pl.loop(0, 5)
-    def _(b):
-        attend(b)
-        inside(b)
+                WN[pl.ds(r0, 128), tile * 128 : (tile + 1) * 128] = mm(WBC[u * 512 + tile * 128 : u * 512 + (tile + 1) * 128, 0:256], xx)
+
+    def two_blocks(h, i):
+        b = h * 4 + 2 * i
+        gate_rows(h, i)
+        for u in range(2):
+            attend(b + u, u)
+            inside(b + u, u)
+
+    @pl.loop(0, 2)
+    def _(i):
+        two_blocks(0, i)
 
     with jax.named_scope("w_s"):
         for j in range(1, nsp):
@@ -490,15 +504,9 @@
         k = lax.rem(me + j, nsp)
         remote(ES.at[k], ER.at[me], es_s.at[k], es_r.at[me], {"sp": k}).start()
 
-    @pl.loop(5, NB)
-    def _(b):
-        attend(b)
-        inside(b)
-
-    with jax.named_scope("c_gate"):
-        for h in range(2):
-            for n in range(2):
-                gate_tile(h, n)
+    @pl.loop(0, 2)
+    def _(i):
+        two_blocks(1, i)
 
     with jax.named_scope("w_e"):
         for j in range(1, nsp):

time: 47.2 us -> 46.3 us (0.981)
  Pallas kernels: 45.8 us -> 44.9 us
    pallas_call x1, Pallas kernels: 45.8 us -> 44.9 us  [local(): pl.pallas_call(lambda *refs: kernel(nsp, *refs), name='layer', out_shape=...]
where the time goes in v3:
time: 46.3 us; the launch traced here: 46.2 us
  Pallas kernels  44.9 us (97%)
  local copies, waits for them, and re-layouts  1.32 us (3%)
    pallas_call x1, Pallas kernels, local(): pl.pallas_call(lambda *refs: kernel(nsp, *refs), name='layer', out_shape=...  44.9 us
    unnamed x1, local copies, waits for them, and re-layouts  1.32 us

profile of v3, /device:TPU:1, one launch (start us, length us, event | category | flops | bytes accessed | tf_op | source)
XLA Modules:
  0.0 46.2 jit_solution(7137625696497013772)
XLA Ops:
  0.0 44.9 %layer.1 = bf16[512,2048]{1,0:T(8,128)(2,1)S(1)} custom-call(bf16[1024,1024]{1,0:T(8,128)(2,1)} %refs_0_.1, f32[1,2048]{1,0:T(1,128)} %bitcast.14, bf16[2048,512]{1,0:T(8,128)(2,1)} %refs_2_.1, bf16[2048,128]{1,0:T(8,128)(2,1)} %refs_3_.1, bf16[2048,128]{1,0:T(8,128)(2,1)} %refs_4_.1, bf16[2048,512]{1,0:T(8,128)(2,1)} %refs_5_.1, bf16[2048,256]{1,0:T(8,128)(2,1)} %refs_6_.1, ...), custom_call_target="tpu_custom_call" | custom-call | tf_op jit(solution)/shard_map/layer/pallas_call | solution.py:630
  44.9 1.3 %copy.27 = bf16[512,2048]{1,0:T(8,128)(2,1)} copy(bf16[512,2048]{1,0:T(8,128)(2,1)S(1)} %layer.1) | data formatting | bytes 4194304
